TPU v7x, 32 devices: a whole 2x2x4 slice. The times are simulated.
32 devices in a mesh: ep: 8 (over z, x), tp: 4 (over y, core).
Axes of the slice: x: 2, y: 2, z: 4, core: 2. Of those that a mesh axis runs over, the one named last changes fastest.
Arguments:
- mixer_input: bfloat16 [1024, 2048], P('ep'), may hold values from -6 to 6
- mixer_gain: bfloat16 [2048], replicated, may hold values from 0.099609375 to 1.8984375
- query_matrix: bfloat16 [2048, 2048], P(None, 'tp'), may hold values from -0.125 to 0.125
- key_matrix: bfloat16 [2048, 2048], P(None, 'tp'), may hold values from -0.125 to 0.125
- value_matrix: bfloat16 [2048, 2048], P(None, 'tp'), may hold values from -0.125 to 0.125
- decay_down_factor: bfloat16 [2048, 64], replicated, may hold values from -0.125 to 0.125
- decay_up_factor: bfloat16 [64, 2048], P(None, 'tp'), may hold values from -1.1953125 to 1.1953125
- decay_bias_base: float32 [2048], P('tp'), may hold values from -16 to 0
- decay_shift: float32 [1024, 2048], P('ep', 'tp'), may hold values from -1.5 to 1.5
- decay_spike: float32 [1024, 2048], P('ep', 'tp'), may hold values from -1.4 to 0
- correction_rate_down: bfloat16 [2048, 64], replicated, may hold values from -0.125 to 0.125
- correction_rate_up: bfloat16 [64, 2048], P(None, 'tp'), may hold values from -1.1953125 to 1.1953125
- correction_rate_base: float32 [2048], P('tp'), may hold values from -8 to 1
- head_norm_gain: bfloat16 [2048], P('tp'), may hold values from 0.099609375 to 1.8984375
- output_weight: bfloat16 [2048, 2048], P('tp'), may hold values from -0.125 to 0.125
- feedforward_input: bfloat16 [2048, 2048], P(('ep', 'tp')), may hold values from -6 to 6
- feedforward_gain: bfloat16 [2048], replicated, may hold values from 0.099609375 to 1.8984375
- routed_expert_index: int32 [2048, 2], P('ep'), may hold values from 0 to 15, all different within a row; in each aligned block of 64 rows (0 to 63, 64 to 127, ...) at most 12 rows name the same one
- routed_expert_weight: float32 [2048, 2], P(('ep', 'tp')), may hold values from 0.3 to 2.5
- expert_gate_weight: bfloat16 [16, 2048, 1024], P('ep', None, 'tp'), may hold values from -0.125 to 0.125
- expert_up_weight: bfloat16 [16, 2048, 1024], P('ep', None, 'tp'), may hold values from -0.125 to 0.125
- expert_down_weight: bfloat16 [16, 1024, 2048], P('ep', 'tp'), may hold values from -0.1875 to 0.1875
- shared_gate_weight: bfloat16 [2048, 1024], P(None, 'tp'), may hold values from -0.125 to 0.125
- shared_up_weight: bfloat16 [2048, 1024], P(None, 'tp'), may hold values from -0.125 to 0.125
- shared_down_weight: bfloat16 [1024, 2048], P('tp'), may hold values from -0.1875 to 0.1875
Outputs:
- mixed_a: bfloat16 [1024, 2048], P(('ep', 'tp'))
- mixed_b: bfloat16 [2048, 2048], P(('ep', 'tp'))
Inputs may be any that keep to these rules, and one draw needn't show every extreme that they name: `routed_expert_index`: in each aligned block of 64 rows (the rows of one device) a row names 2 different experts and no expert is named more than 12 times; in every draw some block names some expert exactly 12 times.
All inputs are finite; a program needn't handle non-finite values.
Results may differ from a plain program's by a relative error of at most 0.017.
Values may be sent and summed in bfloat16 or wider, within the bound.
A program may use at most 128 MiB of HBM per device.

v0:
```python
import jax
import jax.numpy as jnp
from jax import lax
from jax.sharding import PartitionSpec as P

HEAD = 64
TOP = 2
SPAN = 32


highest = lax.Precision.HIGHEST
norm_eps = 1e-06
group_eps = 0.00064
unit_eps = 1e-06


def entering(shard, axis, combine, identity):
    size, place = (lax.axis_size(axis), lax.axis_index(axis))
    everything = jax.tree.map(
        lambda part, kind: lax.all_gather(part.astype(kind), axis),
        shard,
        (jnp.bfloat16, jnp.bfloat16),
    )
    start = jax.tree.map(
        lambda part, zero: jnp.broadcast_to(jnp.asarray(zero, part.dtype), part.shape),
        shard,
        identity,
    )

    def hop(k, before):
        reached = k < place
        new = combine(
            before, jax.tree.map(lambda part, own: part[k].astype(own.dtype), everything, shard)
        )
        return jax.tree.map(lambda a, b: jnp.where(reached, a, b), new, before)

    return lax.fori_loop(0, size, hop, start)


def rms_rows(matrix, gain):
    values = matrix.astype(jnp.float32)
    scaled = values * lax.rsqrt(jnp.mean(values * values, axis=-1, keepdims=True) + norm_eps)
    return (scaled * gain.astype(jnp.float32)).astype(jnp.bfloat16)


def mixer_channel_rows(
    normed_rows,
    query_matrix,
    key_matrix,
    value_matrix,
    decay_down_factor,
    decay_up_factor,
    decay_bias_base,
    decay_shift,
    decay_spike,
    correction_rate_down,
    correction_rate_up,
    correction_rate_base,
):
    row_count = normed_rows.shape[0]
    head_count = query_matrix.shape[1] // HEAD

    def by_heads(matrix):
        return matrix.reshape(row_count, head_count, HEAD)

    query_matrix_rows = jnp.dot(normed_rows, query_matrix, preferred_element_type=jnp.float32)
    key_matrix_rows = jnp.dot(normed_rows, key_matrix, preferred_element_type=jnp.float32)
    value_matrix_rows = jnp.dot(normed_rows, value_matrix, preferred_element_type=jnp.float32)
    decay_low = jnp.tanh(
        jnp.dot(normed_rows, decay_down_factor, preferred_element_type=jnp.float32)
    ).astype(jnp.bfloat16)
    decay_logits = (
        decay_bias_base
        + jnp.dot(decay_low, decay_up_factor, preferred_element_type=jnp.float32)
        + decay_shift
    )
    logarithm_decay = decay_spike - jnp.exp(-jax.nn.softplus(-decay_logits) - 0.5)
    iclr_low = jnp.dot(
        normed_rows, correction_rate_down, preferred_element_type=jnp.float32
    ).astype(jnp.bfloat16)
    learning = jax.nn.sigmoid(
        correction_rate_base
        + jnp.dot(iclr_low, correction_rate_up, preferred_element_type=jnp.float32)
    )
    key_matrix_rows = by_heads(key_matrix_rows)
    unit_keys = key_matrix_rows * lax.rsqrt(
        jnp.sum(key_matrix_rows * key_matrix_rows, axis=-1, keepdims=True) + unit_eps
    )
    return (
        by_heads(query_matrix_rows),
        key_matrix_rows,
        by_heads(value_matrix_rows),
        -unit_keys,
        unit_keys * by_heads(learning),
        by_heads(logarithm_decay),
    )


def head_norm(outputs, gain):
    row_mean = jnp.mean(outputs, axis=-1, keepdims=True)
    centered = outputs - row_mean
    row_var = jnp.mean(centered * centered, axis=-1, keepdims=True)
    scaled = (centered * lax.rsqrt(row_var + group_eps)).reshape(outputs.shape[0], -1)
    return (scaled * gain.astype(jnp.float32)).astype(jnp.bfloat16)


def block_tables(query_matrix_rows, key_matrix_rows, erase_vector, write_vector, logarithm_decay):
    length = query_matrix_rows.shape[1]
    cumulative = jnp.cumsum(logarithm_decay, axis=1)
    before_decay = cumulative - logarithm_decay
    position = jnp.arange(length)
    strictly_below = (position[:, None] > position[None, :])[None, :, :, None]
    up_to = (position[:, None] >= position[None, :])[None, :, :, None]
    fade_before = jnp.exp(
        jnp.where(strictly_below, before_decay[:, :, None, :] - cumulative[:, None, :, :], -jnp.inf)
    )
    fade_upto = jnp.exp(
        jnp.where(up_to, cumulative[:, :, None, :] - cumulative[:, None, :, :], -jnp.inf)
    )
    erase_write = jnp.einsum(
        "htc,htsc,hsc->hts", erase_vector, fade_before, write_vector, precision=highest
    )
    erase_key = jnp.einsum(
        "htc,htsc,hsc->hts", erase_vector, fade_before, key_matrix_rows, precision=highest
    )
    query_write = jnp.einsum(
        "htc,htsc,hsc->hts", query_matrix_rows, fade_upto, write_vector, precision=highest
    )
    query_key = jnp.einsum(
        "htc,htsc,hsc->hts", query_matrix_rows, fade_upto, key_matrix_rows, precision=highest
    )
    identity = jnp.broadcast_to(jnp.eye(length, dtype=jnp.float32), erase_write.shape)
    inverse = jax.scipy.linalg.solve_triangular(
        identity - erase_write, identity, lower=True, unit_diagonal=True
    )
    to_end = jnp.exp(cumulative[:, -1:, :] - cumulative)
    return (
        inverse,
        erase_key,
        query_write,
        query_key,
        jnp.exp(before_decay) * erase_vector,
        jnp.exp(cumulative) * query_matrix_rows,
        to_end * write_vector,
        to_end * key_matrix_rows,
        jnp.exp(cumulative[:, -1, :]),
    )


def advance_block(carried, tables, block_values, with_output):
    (
        inverse,
        erase_key,
        query_write,
        query_key,
        start_erase,
        start_query,
        end_write,
        end_key,
        end_fade,
    ) = tables
    right_side = jnp.einsum("htk,hpk->htp", start_erase, carried, precision=highest) + jnp.einsum(
        "hts,hsp->htp", erase_key, block_values, precision=highest
    )
    held = jnp.einsum("hts,hsp->htp", inverse, right_side, precision=highest)
    next_state = (
        carried * end_fade[:, None, :]
        + jnp.einsum("htp,htk->hpk", held, end_write, precision=highest)
        + jnp.einsum("htp,htk->hpk", block_values, end_key, precision=highest)
    )
    if not with_output:
        return (next_state, None)
    output = (
        jnp.einsum("htk,hpk->htp", start_query, carried, precision=highest)
        + jnp.einsum("hts,hsp->htp", query_write, held, precision=highest)
        + jnp.einsum("hts,hsp->htp", query_key, block_values, precision=highest)
    )
    return (next_state, output)


def chain(earlier, later):
    product = jnp.einsum("hij,hjk->hik", earlier[0], later[0], precision=highest)
    added = jnp.einsum("hij,hjk->hik", earlier[1], later[0], precision=highest) + later[1]
    return (product, added)


def slot_positions(route_block, experts):
    flat_ids = route_block.reshape(-1)
    onehot = (flat_ids[:, None] == jnp.arange(experts, dtype=jnp.int32)[None, :]).astype(jnp.int32)
    earlier_count = jnp.cumsum(onehot, axis=0) - onehot
    return jnp.sum(earlier_count * onehot, axis=1).reshape(route_block.shape)


def per_device(
    mixer_input,
    mixer_gain,
    query_matrix,
    key_matrix,
    value_matrix,
    decay_down_factor,
    decay_up_factor,
    decay_bias_base,
    decay_shift,
    decay_spike,
    correction_rate_down,
    correction_rate_up,
    correction_rate_base,
    head_norm_gain,
    output_weight,
    feedforward_input,
    feedforward_gain,
    routed_expert_index,
    routed_expert_weight,
    expert_gate_weight,
    expert_up_weight,
    expert_down_weight,
    shared_gate_weight,
    shared_up_weight,
    shared_down_weight,
):
    tp_size = lax.axis_size("tp")
    ep_size = lax.axis_size("ep")
    normed_first = rms_rows(mixer_input, mixer_gain)
    (
        query_matrix_rows,
        key_matrix_rows,
        value_matrix_rows,
        erase_vector,
        write_vector,
        logarithm_decay,
    ) = mixer_channel_rows(
        normed_first,
        query_matrix,
        key_matrix,
        value_matrix,
        decay_down_factor,
        decay_up_factor,
        decay_bias_base,
        decay_shift,
        decay_spike,
        correction_rate_down,
        correction_rate_up,
        correction_rate_base,
    )
    row_count, head_count, head_size = query_matrix_rows.shape
    block_count = row_count // SPAN

    def to_blocks(matrix):
        return matrix.reshape(block_count, SPAN, head_count, head_size).transpose(0, 2, 1, 3)

    tables = lax.map(
        lambda block_items: block_tables(*block_items),
        (
            to_blocks(query_matrix_rows),
            to_blocks(key_matrix_rows),
            to_blocks(erase_vector),
            to_blocks(write_vector),
            to_blocks(logarithm_decay),
        ),
    )
    value_blocks = to_blocks(value_matrix_rows)
    identity = jnp.broadcast_to(
        jnp.eye(head_size, dtype=jnp.float32), (head_count, head_size, head_size)
    )
    zero_state = jnp.zeros((head_count, head_size, head_size), jnp.float32)

    def state_only(carried, block_items):
        block_table, block_values = block_items
        widened = jnp.concatenate([block_values, jnp.zeros_like(block_values)], axis=2)
        return (advance_block(carried, block_table, widened, False)[0], None)

    final_state, _ = lax.scan(
        state_only, jnp.concatenate([zero_state, identity], axis=1), (tables, value_blocks)
    )
    _, incoming = entering(
        (final_state[:, head_size:], final_state[:, :head_size]),
        "ep",
        chain,
        (identity, zero_state),
    )

    def with_output(carried, block_items):
        block_table, block_values = block_items
        return advance_block(carried, block_table, block_values, True)

    _, head_out = lax.scan(with_output, incoming, (tables, value_blocks))
    head_out = head_out.transpose(0, 2, 1, 3).reshape(row_count, head_count, head_size)
    mixed_rows = head_norm(head_out, head_norm_gain)
    mixed_a = lax.psum_scatter(
        jnp.dot(mixed_rows, output_weight, preferred_element_type=jnp.float32).astype(jnp.bfloat16),
        "tp",
        scatter_dimension=0,
        tiled=True,
    )
    own_count = feedforward_input.shape[0]
    local_count = expert_gate_weight.shape[0]
    experts = local_count * ep_size
    capacity = max(2, 3 * own_count * TOP // (2 * experts))
    normed_own = rms_rows(feedforward_input, feedforward_gain)
    model_width = normed_own.shape[1]
    group_rows = lax.all_gather(normed_own, "tp", axis=0, tiled=True)
    own_ids = lax.dynamic_slice_in_dim(
        routed_expert_index, lax.axis_index("tp") * own_count, own_count, 0
    )
    own_positions = slot_positions(own_ids, experts)
    zero_row = jnp.zeros((1, model_width), jnp.bfloat16)
    slot_index = own_ids * capacity + own_positions
    slot_table = jnp.full((experts * capacity,), own_count, jnp.int32)
    slot_table = slot_table.at[slot_index.reshape(-1)].set(
        jnp.broadcast_to(jnp.arange(own_count, dtype=jnp.int32)[:, None], slot_index.shape).reshape(
            -1
        )
    )
    padded = jnp.concatenate([normed_own, zero_row], axis=0)
    outgoing = padded[slot_table].reshape(experts, capacity, model_width)
    received = lax.all_to_all(outgoing, "ep", split_axis=0, concat_axis=0, tiled=True)
    arrived = lax.all_gather(received[None], "tp", axis=0, tiled=True)
    arrived = arrived.reshape(tp_size, ep_size, local_count, capacity, model_width)
    gate_out = jnp.einsum(
        "tgjcd,jdf->tgjcf", arrived, expert_gate_weight, preferred_element_type=jnp.float32
    )
    up_out = jnp.einsum(
        "tgjcd,jdf->tgjcf", arrived, expert_up_weight, preferred_element_type=jnp.float32
    )
    hidden = (jax.nn.silu(gate_out) * up_out).astype(jnp.bfloat16)
    shared_hidden = (
        jax.nn.silu(jnp.dot(group_rows, shared_gate_weight, preferred_element_type=jnp.float32))
        * jnp.dot(group_rows, shared_up_weight, preferred_element_type=jnp.float32)
    ).astype(jnp.bfloat16)
    shared_hidden = shared_hidden.reshape(tp_size, own_count, -1)
    routed_rows = ep_size * local_count * capacity
    block_rows = routed_rows + own_count
    block_total = lax.axis_size("tp") * block_rows // block_rows
    routed_part = jnp.einsum(
        "tgjcf,jfd->tgjcd", hidden, expert_down_weight, preferred_element_type=jnp.float32
    )
    shared_part = jnp.einsum(
        "tnf,fd->tnd", shared_hidden, shared_down_weight, preferred_element_type=jnp.float32
    )
    joined = jnp.concatenate(
        [routed_part.reshape(block_total, routed_rows, model_width), shared_part], axis=1
    )
    summed = lax.psum_scatter(
        joined.reshape(lax.axis_size("tp") * block_rows, model_width).astype(jnp.bfloat16),
        "tp",
        scatter_dimension=0,
        tiled=True,
    ).astype(jnp.float32)
    expert_out = (
        summed[:routed_rows]
        .astype(jnp.bfloat16)
        .reshape(ep_size, local_count * capacity, model_width)
    )
    returned = lax.all_to_all(expert_out, "ep", split_axis=0, concat_axis=0, tiled=True).reshape(
        experts * capacity, model_width
    )
    picked = returned[own_ids * capacity + own_positions]
    routed = jnp.einsum(
        "rk,rkd->rd", routed_expert_weight, picked.astype(jnp.float32), precision=highest
    )
    mixed_b = (routed + summed[routed_rows:]).astype(jnp.bfloat16)
    return (mixed_a, mixed_b)


def solution(mesh):
    in_specs = (
        P("ep", None),
        P(),
        P(None, "tp"),
        P(None, "tp"),
        P(None, "tp"),
        P(),
        P(None, "tp"),
        P("tp"),
        P("ep", "tp"),
        P("ep", "tp"),
        P(),
        P(None, "tp"),
        P("tp"),
        P("tp"),
        P("tp", None),
        P(("ep", "tp"), None),
        P(),
        P("ep", None),
        P(("ep", "tp"), None),
        P("ep", None, "tp"),
        P("ep", None, "tp"),
        P("ep", "tp", None),
        P(None, "tp"),
        P(None, "tp"),
        P("tp", None),
    )
    out_specs = (P(("ep", "tp"), None), P(("ep", "tp"), None))
    return jax.shard_map(
        per_device, mesh=mesh, in_specs=in_specs, out_specs=out_specs, check_vma=False
    )
```

profile of v0, /device:TPU:0, one launch (start us, length us, event | category | flops | bytes accessed | tf_op | source)
XLA Modules:
  0.0 554.6 jit_solution(11777558396313947492)
XLA Ops:
  19.7 7.3 %all-to-all-start = ((bf16[16,12,2048]{2,1,0:T(8,128)(2,1)}), bf16[16,12,2048]{2,1,0:T(8,128)(2,1)}, u32[]{:S(2)}, u32[]{:S(2)}) async-start(bf16[16,12,2048]{2,1,0:T(8,128)(2,1)} %reshape.226), calls=%async_computation.1 | async-start | bytes 2097152 | tf_op jit(solution)/shard_map/all_to_all | solution.py:316
  40.8 12.1 %all-to-all-done = bf16[16,12,2048]{2,1,0:T(8,128)(2,1)} async-done(((bf16[16,12,2048]{2,1,0:T(8,128)(2,1)}), bf16[16,12,2048]{2,1,0:T(8,128)(2,1)}, u32[]{:S(2)}, u32[]{:S(2)}) %all-to-all-start) | async-done | bytes 786464 | tf_op jit(solution)/shard_map/all_to_all | solution.py:316
  58.1 244.8 %while.62 = (s32[]{:T(128)}, f32[4,8,32,32]{3,2,1,0:T(8,128)}, f32[4,8,32,32]{3,2,1,0:T(8,128)}, f32[4,8,32,32]{3,2,1,0:T(8,128)}, f32[4,8,32,32]{3,2,1,0:T(8,12...) while((s32[]{:T(128)}, f32[4,8,32,32]{3,2,1,0:T(8,128)}, ...), condition=%wide.region_4.5_spmd, body=%wide.region_2.4_spmd.sunk | while | flops 35257376 | bytes 4666261 | solution.py:251
  76.5 7.3 %fusion.287 = f32[8,32,1,32]{3,2,1,0:T(1,128)S(1)} fusion(f32[8,32,64]{2,1,0:T(8,128)S(1)} %copy.228, f32[8,32,64]{2,1,0:T(8,128)S(1)} %bitcast.352, pred[32,32]{1,0:T(8,128)(4,1)S(1)} %iota_compare_fusion.12, f32[8,32,64,1]{2,0,1,3:T(8,128)S(1)} %get-tuple-element.846), kind=kOutput, calls=%fused_computation.5.clone.1 | convolution fusion | flops 7864320 | bytes 230400 | tf_op jit(solution)/shard_map/while/body/eval_jaxpr/htc,htsc,hsc->hts/dot_general | solution.py:126
  83.8 7.3 %fusion.286 = f32[8,32,1,32]{3,2,1,0:T(1,128)S(1)} fusion(f32[8,32,64]{2,1,0:T(8,128)S(1)} %copy.228, f32[8,32,64]{2,1,0:T(8,128)S(1)} %bitcast.354, pred[32,32]{1,0:T(8,128)(4,1)S(1)} %iota_compare_fusion.12, f32[8,32,64,1]{2,0,1,3:T(8,128)S(1)} %get-tuple-element.846), kind=kOutput, calls=%fused_computation.3.clone.1 | convolution fusion | flops 7864320 | bytes 230400 | tf_op jit(solution)/shard_map/while/body/eval_jaxpr/htc,htsc,hsc->hts/dot_general | solution.py:129
  92.6 7.3 %fusion.285 = f32[8,32,1,32]{3,2,1,0:T(1,128)S(1)} fusion(f32[8,32,64]{2,1,0:T(8,128)S(1)} %bitcast.355, f32[8,32,64]{2,1,0:T(8,128)S(1)} %copy.228, f32[8,32,64]{2,1,0:T(8,128)S(1)} %copy.229, pred[32,32]{1,0:T(8,128)(4,1)S(1)} %iota_compare_fusion.10, f32[8,32,64,1]{2,0,1,3:T(8,128)S(1)} %get-tuple-element.842), kind=kOutput, calls=%fused_computation.7.clone.1 | convolution fusion | flops 7864320 | bytes 295936 | tf_op jit(solution)/shard_map/while/body/eval_jaxpr/htc,htsc,hsc->hts/dot_general | solution.py:123
  108.0 20.3 %custom-call.16 = f32[8,1,32,32]{2,3,1,0:T(8,128)} custom-call(f32[8,1,32,32]{3,2,1,0:T(8,128)S(1)} %add_bitcast_fusion.2), custom_call_target="InvertDiagBlocksLowerTriangular" | custom-call | tf_op jit(solution)/shard_map/while/body/eval_jaxpr/jit(_solve_triangular)/vmap()/triangular_solve | solution.py:133
  140.8 7.3 %fusion.286 = f32[8,32,1,32]{3,2,1,0:T(1,128)S(1)} fusion(f32[8,32,64]{2,1,0:T(8,128)S(1)} %copy.228, f32[8,32,64]{2,1,0:T(8,128)S(1)} %bitcast.354, pred[32,32]{1,0:T(8,128)(4,1)S(1)} %iota_compare_fusion.12, f32[8,32,64,1]{2,0,1,3:T(8,128)S(1)} %get-tuple-element.846), kind=kOutput, calls=%fused_computation.3.clone.1 | convolution fusion | flops 7864320 | bytes 230400 | tf_op jit(solution)/shard_map/while/body/eval_jaxpr/htc,htsc,hsc->hts/dot_general | solution.py:129
  149.6 7.3 %fusion.285 = f32[8,32,1,32]{3,2,1,0:T(1,128)S(1)} fusion(f32[8,32,64]{2,1,0:T(8,128)S(1)} %bitcast.355, f32[8,32,64]{2,1,0:T(8,128)S(1)} %copy.228, f32[8,32,64]{2,1,0:T(8,128)S(1)} %copy.229, pred[32,32]{1,0:T(8,128)(4,1)S(1)} %iota_compare_fusion.10, f32[8,32,64,1]{2,0,1,3:T(8,128)S(1)} %get-tuple-element.842), kind=kOutput, calls=%fused_computation.7.clone.1 | convolution fusion | flops 7864320 | bytes 295936 | tf_op jit(solution)/shard_map/while/body/eval_jaxpr/htc,htsc,hsc->hts/dot_general | solution.py:123
  165.0 20.3 %custom-call.16 = f32[8,1,32,32]{2,3,1,0:T(8,128)} custom-call(f32[8,1,32,32]{3,2,1,0:T(8,128)S(1)} %add_bitcast_fusion.2), custom_call_target="InvertDiagBlocksLowerTriangular" | custom-call | tf_op jit(solution)/shard_map/while/body/eval_jaxpr/jit(_solve_triangular)/vmap()/triangular_solve | solution.py:133
  190.5 7.3 %fusion.287 = f32[8,32,1,32]{3,2,1,0:T(1,128)S(1)} fusion(f32[8,32,64]{2,1,0:T(8,128)S(1)} %copy.228, f32[8,32,64]{2,1,0:T(8,128)S(1)} %bitcast.352, pred[32,32]{1,0:T(8,128)(4,1)S(1)} %iota_compare_fusion.12, f32[8,32,64,1]{2,0,1,3:T(8,128)S(1)} %get-tuple-element.846), kind=kOutput, calls=%fused_computation.5.clone.1 | convolution fusion | flops 7864320 | bytes 230400 | tf_op jit(solution)/shard_map/while/body/eval_jaxpr/htc,htsc,hsc->hts/dot_general | solution.py:126
  197.8 7.3 %fusion.286 = f32[8,32,1,32]{3,2,1,0:T(1,128)S(1)} fusion(f32[8,32,64]{2,1,0:T(8,128)S(1)} %copy.228, f32[8,32,64]{2,1,0:T(8,128)S(1)} %bitcast.354, pred[32,32]{1,0:T(8,128)(4,1)S(1)} %iota_compare_fusion.12, f32[8,32,64,1]{2,0,1,3:T(8,128)S(1)} %get-tuple-element.846), kind=kOutput, calls=%fused_computation.3.clone.1 | convolution fusion | flops 7864320 | bytes 230400 | tf_op jit(solution)/shard_map/while/body/eval_jaxpr/htc,htsc,hsc->hts/dot_general | solution.py:129
  206.6 7.3 %fusion.285 = f32[8,32,1,32]{3,2,1,0:T(1,128)S(1)} fusion(f32[8,32,64]{2,1,0:T(8,128)S(1)} %bitcast.355, f32[8,32,64]{2,1,0:T(8,128)S(1)} %copy.228, f32[8,32,64]{2,1,0:T(8,128)S(1)} %copy.229, pred[32,32]{1,0:T(8,128)(4,1)S(1)} %iota_compare_fusion.10, f32[8,32,64,1]{2,0,1,3:T(8,128)S(1)} %get-tuple-element.842), kind=kOutput, calls=%fused_computation.7.clone.1 | convolution fusion | flops 7864320 | bytes 295936 | tf_op jit(solution)/shard_map/while/body/eval_jaxpr/htc,htsc,hsc->hts/dot_general | solution.py:123
  222.0 20.3 %custom-call.16 = f32[8,1,32,32]{2,3,1,0:T(8,128)} custom-call(f32[8,1,32,32]{3,2,1,0:T(8,128)S(1)} %add_bitcast_fusion.2), custom_call_target="InvertDiagBlocksLowerTriangular" | custom-call | tf_op jit(solution)/shard_map/while/body/eval_jaxpr/jit(_solve_triangular)/vmap()/triangular_solve | solution.py:133
  247.5 7.3 %fusion.287 = f32[8,32,1,32]{3,2,1,0:T(1,128)S(1)} fusion(f32[8,32,64]{2,1,0:T(8,128)S(1)} %copy.228, f32[8,32,64]{2,1,0:T(8,128)S(1)} %bitcast.352, pred[32,32]{1,0:T(8,128)(4,1)S(1)} %iota_compare_fusion.12, f32[8,32,64,1]{2,0,1,3:T(8,128)S(1)} %get-tuple-element.846), kind=kOutput, calls=%fused_computation.5.clone.1 | convolution fusion | flops 7864320 | bytes 230400 | tf_op jit(solution)/shard_map/while/body/eval_jaxpr/htc,htsc,hsc->hts/dot_general | solution.py:126
  254.8 7.3 %fusion.286 = f32[8,32,1,32]{3,2,1,0:T(1,128)S(1)} fusion(f32[8,32,64]{2,1,0:T(8,128)S(1)} %copy.228, f32[8,32,64]{2,1,0:T(8,128)S(1)} %bitcast.354, pred[32,32]{1,0:T(8,128)(4,1)S(1)} %iota_compare_fusion.12, f32[8,32,64,1]{2,0,1,3:T(8,128)S(1)} %get-tuple-element.846), kind=kOutput, calls=%fused_computation.3.clone.1 | convolution fusion | flops 7864320 | bytes 230400 | tf_op jit(solution)/shard_map/while/body/eval_jaxpr/htc,htsc,hsc->hts/dot_general | solution.py:129
  278.9 20.3 %custom-call.16 = f32[8,1,32,32]{2,3,1,0:T(8,128)} custom-call(f32[8,1,32,32]{3,2,1,0:T(8,128)S(1)} %add_bitcast_fusion.2), custom_call_target="InvertDiagBlocksLowerTriangular" | custom-call | tf_op jit(solution)/shard_map/while/body/eval_jaxpr/jit(_solve_triangular)/vmap()/triangular_solve | solution.py:133
  325.1 7.9 %convert_bitcast_fusion = bf16[4,8,2,12,2048]{4,3,1,0,2:T(8,128)(2,1)} fusion(bf16[2,256,2048]{2,1,0:T(8,128)(2,1)S(1)} %copy-done, bf16[2,2048,256]{2,1,0:T(8,128)(2,1)} %param.53, bf16[4,8,2,12,2048]{4,2,1,0,3:T(2,128)(2,1)} %reshape.227, f32[4,8,2,12,256]{4,3,1,0,2:T(8,128)} %fusion.127), kind=kOutput, calls=%fused_computation.170 | convolution fusion | flops 1613365248 | bytes 11272192 | tf_op jit(solution)/shard_map/tgjcf,jfd->tgjcd/dot_general | solution.py:334
  345.9 27.1 %while.63 = (s32[]{:T(128)}, f32[8,128,64]{1,2,0:T(8,128)S(1)}, f32[4,8,64]{2,1,0:T(8,128)S(1)}, f32[4,8,32,32]{3,2,1,0:T(8,128)}, f32[4,8,32,64]{3,2,1,0:T(8,12...) while((s32[]{:T(128)}, f32[8,128,64]{1,2,0:T(8,128)S(1)}, ...), condition=%wide.region_6.7_spmd, body=%wide.region_5.6_spmd.sunk | while | flops 100892672 | bytes 3023469 | solution.py:272
  373.2 35.0 %all-gather = bf16[64,64,64]{2,1,0:T(8,128)(2,1)} all-gather(bf16[8,64,64]{2,1,0:T(8,128)(2,1)S(1)} %get-tuple-element.591), channel_id=2, replica_groups=mesh['ep'=8,'tp'=4] {'ep'}, dimensions={0}, use_global_device_ids=true | all-gather | bytes 589824 | tf_op jit(solution)/shard_map/all_gather | solution.py:20
  408.2 34.7 %all-gather.1 = bf16[64,64,64]{2,1,0:T(8,128)(2,1)} all-gather(bf16[8,64,64]{2,1,0:T(8,128)(2,1)S(1)} %get-tuple-element.590), channel_id=3, replica_groups=mesh['ep'=8,'tp'=4] {'ep'}, dimensions={0}, use_global_device_ids=true | all-gather | bytes 589824 | tf_op jit(solution)/shard_map/all_gather | solution.py:20
  442.9 18.6 %while.65 = (s32[]{:T(128)}, f32[8,64,64]{1,2,0:T(8,128)S(1)}, s32[]{:T(128)}, bf16[8,8,64,64]{3,2,1,0:T(8,128)(2,1)}, bf16[8,8,64,64]{3,2,1,0:T(8,128)(2,1)}, /*index=5*/s32[]{:T(128)}, s32[]{:T(128)}) while((s32[]{:T(128)}, f32[8,64,64]{1,2,0:T(8,128)S(1)}, s32[]{:T(128)}, bf16[8,8,64,64]{3,2,1,0:T(8,128)(2,1)}, ...), condition=%wide.region_8.9_spmd.clone, body=%wide.region_7.8_spmd.clone.sunk | while | flops 25329668 | bytes 1443939 | solution.py:37
  468.4 46.0 %while.64 = (s32[]{:T(128)}, f32[8,64,64]{2,1,0:T(8,128)S(1)}, f32[4,8,32,64]{3,2,1,0:T(8,128)}, f32[4,8,64]{2,1,0:T(8,128)S(1)}, f32[4,8,32,32]{3,2,1,0:T(8,128...) while((s32[]{:T(128)}, f32[8,64,64]{2,1,0:T(8,128)S(1)}, ...), condition=%wide.region_10.11_spmd, body=%wide.region_9.10_spmd.sunk | while | flops 75644928 | bytes 3157645 | solution.py:286
  529.7 18.1 %reduce-scatter.3.cloned.1.call-done = bf16[32,2048]{1,0:T(8,128)(2,1)} async-done(((bf16[128,2048]{1,0:T(8,128)(2,1)}), bf16[32,2048]{1,0:T(8,128)(2,1)}) %reduce-scatter.3.cloned.1.call-update) | async-done | bytes 131088 | tf_op jit(solution)/shard_map/reduce_scatter | solution.py:289
  (315 shorter events, 252.7 us)
Async XLA Ops:
  7.2 318.0 %copy-start = (bf16[2,256,2048]{2,1,0:T(8,128)(2,1)S(1)}, bf16[2,256,2048]{2,1,0:T(8,128)(2,1)}, u32[]{:S(2)}) copy-start(bf16[2,256,2048]{2,1,0:T(8,128)(2,1)} %param.54) | copy-start | bytes 6291460
  7.2 299.9 %all-gather.6.cloned.1.call-start = ((), (), s32[]{:S(2)}) async-start(), calls=%async_computation.5 | async-start | bytes 1310720 | tf_op jit(solution)/shard_map/all_gather | solution.py:301
  15.5 11.6 %copy-start.9 = (bf16[2048]{0:T(1024)(128)(2,1)S(1)}, bf16[2048]{0:T(1024)(128)(2,1)}, u32[]{:S(2)}) copy-start(bf16[2048]{0:T(1024)(128)(2,1)} %param.34) | copy-start | bytes 12292
  15.5 11.6 %copy-start.2 = (bf16[128,2048]{1,0:T(8,128)(2,1)S(1)}, bf16[128,2048]{1,0:T(8,128)(2,1)}, u32[]{:S(2)}) copy-start(bf16[128,2048]{1,0:T(8,128)(2,1)} %param.33) | copy-start | bytes 1572868
  17.6 13.1 %copy-start.12 = (bf16[64,512]{1,0:T(8,128)(2,1)S(1)}, bf16[64,512]{1,0:T(8,128)(2,1)}, u32[]{:S(2)}) copy-start(bf16[64,512]{1,0:T(8,128)(2,1)} %param.44) | copy-start | bytes 196612
  17.6 13.1 %copy-start.13 = (f32[512]{0:T(512)S(1)}, f32[512]{0:T(512)}, u32[]{:S(2)}) copy-start(f32[512]{0:T(512)} %param.45) | copy-start | bytes 6148
  19.7 33.2 %all-to-all-start = ((bf16[16,12,2048]{2,1,0:T(8,128)(2,1)}), bf16[16,12,2048]{2,1,0:T(8,128)(2,1)}, u32[]{:S(2)}, u32[]{:S(2)}) async-start(bf16[16,12,2048]{2,1,0:T(8,128)(2,1)} %reshape.226), calls=%async_computation.1 | async-start | bytes 2097152 | tf_op jit(solution)/shard_map/all_to_all | solution.py:316
  27.0 286.4 %all-gather.8.cloned.1.call-start = ((), (), s32[]{:S(2)}) async-start(), calls=%async_computation.7 | async-start | bytes 3932160 | tf_op jit(solution)/shard_map/all_gather | solution.py:317
  27.1 8.2 %copy-start.5 = (f32[2048]{0:T(1024)}, f32[2048]{0:T(1024)S(1)}, u32[]{:S(2)}) copy-start(f32[2048]{0:T(1024)S(1)} %convert_element_type.77) | copy-start | bytes 24580
  27.3 8.0 %copy-start.8 = (f32[128]{0:T(128)}, f32[128]{0:T(128)S(1)}, u32[]{:S(2)}) copy-start(f32[128]{0:T(128)S(1)} %add_rsqrt_fusion.3) | copy-start | bytes 1540
  55.5 406.3 %reduce-scatter.5.cloned.1.call-start = ((), (), s32[]{:S(2)}) async-start(), calls=%async_computation.6 | async-start | bytes 5242880 | tf_op jit(solution)/shard_map/reduce_scatter | solution.py:343
  307.1 4.1 copy-start.4
  333.1 5.0 copy-start.3
  345.2 0.7 copy-start.7
  373.0 69.9 %copy-start.1 = (f32[4,8,32,64]{3,2,1,0:T(8,128)}, f32[4,8,32,64]{3,2,1,0:T(8,128)S(1)}, u32[]{:S(2)}) copy-start(f32[4,8,32,64]{3,2,1,0:T(8,128)S(1)} %get-tuple-element.1028) | copy-start | bytes 786436
  463.8 60.9 %all-to-all-start.1 = ((bf16[8,24,2048]{2,1,0:T(8,128)(2,1)}), bf16[8,24,2048]{2,1,0:T(8,128)(2,1)S(1)}, u32[]{:S(2)}, u32[]{:S(2)}) async-start(bf16[8,24,2048]{2,1,0:T(8,128)(2,1)} %bitcast.357), calls=%async_computation.3 | async-start | bytes 1572864 | tf_op jit(solution)/shard_map/all_to_all | solution.py:354
  467.4 80.4 %reduce-scatter.3.cloned.1.call-start = ((), (), s32[]{:S(2)}) async-start(), calls=%async_computation.4 | async-start | bytes 655360 | tf_op jit(solution)/shard_map/reduce_scatter | solution.py:289
  514.4 7.1 %copy-start.10 = (bf16[512]{0:T(512)(128)(2,1)S(1)}, bf16[512]{0:T(512)(128)(2,1)}, u32[]{:S(2)}) copy-start(bf16[512]{0:T(512)(128)(2,1)} %param.46) | copy-start | bytes 3076
  514.4 10.1 %copy-start.6 = (s32[64,2]{1,0:T(8,128)S(1)}, s32[64,2]{1,0:T(8,128)}, u32[]{:S(2)}) copy-start(s32[64,2]{1,0:T(8,128)} %get-tuple-element.566) | copy-start | bytes 1540
  514.4 10.3 %copy-start.11 = (f32[64,2]{0,1:T(2,128)S(1)}, f32[64,2]{0,1:T(2,128)}, u32[]{:S(2)}) copy-start(f32[64,2]{0,1:T(2,128)} %param.51) | copy-start | bytes 1540
Sparse Core Ops, SparseCore 0:
  11.1 19.4 all-gather.5
  55.6 27.5 all-gather.7
  345.4 43.5 reduce-scatter.4
  524.6 23.1 reduce-scatter.2
where the time goes:
time: 562 us; the launch traced here: 555 us
  matrix products  236 us (42%)
  other arithmetic  104 us (19%)
  local copies, waits for them, and re-layouts  71 us (13%)
  blocking collectives  69.7 us (12%)
  waiting for transfers between devices  30.4 us (5%)
  loops' own time  17.9 us (3%)
  between operations  14.6 us (3%)
  starting transfers between devices  11 us (2%)
    another operation x20, other arithmetic, block_tables(): jax.scipy.linalg.solve_triangular(identity - erase_write, identity, lower...  81.8 us
    all_gather x2, blocking collectives, entering(): lax.all_gather(part.astype(kind), axis)  69.7 us
    dot_general x4, matrix products, block_tables(): jnp.einsum('htc,htsc,hsc->hts', query_matrix_rows, fade_upto, key_matrix_...  29.1 us
    dot_general x4, matrix products, block_tables(): jnp.einsum('htc,htsc,hsc->hts', erase_vector, fade_before, key_matrix_row...  29.1 us
    dot_general x4, matrix products, block_tables(): jnp.einsum('htc,htsc,hsc->hts', query_matrix_rows, fade_upto, write_vecto...  29.1 us
    dot_general x4, matrix products, block_tables(): jnp.einsum('htc,htsc,hsc->hts', erase_vector, fade_before, write_vector,...  29.1 us
    reduce_scatter x1, waiting for transfers between devices, per_device(): lax.psum_scatter(jnp.dot(mixed_rows, output_weight, preferred_element_typ...  18.1 us
    another operation x1, loops' own time, per_device(): lax.map(lambda block_items: block_tables(*block_items), (to_blocks(query_...  17 us
  transfers between devices with their start and end apart: 6, of which 2 were waited for; matrix products, arithmetic and copies ran while one was open for 67% of the time, Pallas kernels for 0%

commit v1 on v0

v1 whole, which is shorter than its diff:
```python
import jax
import jax.numpy as jnp
from jax import lax
from jax.experimental import pallas as pl
from jax.experimental.pallas import tpu as pltpu
from jax.sharding import PartitionSpec as P

HEAD = 64
TOP = 2
CHUNK = 64
PAIR = 2


highest = lax.Precision.HIGHEST
norm_eps = 1e-06
group_eps = 0.00064
unit_eps = 1e-06


def rms_rows(matrix, gain):
    values = matrix.astype(jnp.float32)
    scaled = values * lax.rsqrt(jnp.mean(values * values, axis=-1, keepdims=True) + norm_eps)
    return (scaled * gain.astype(jnp.float32)).astype(jnp.bfloat16)


def mixer_channel_rows(
    normed_rows,
    query_matrix,
    key_matrix,
    value_matrix,
    decay_down_factor,
    decay_up_factor,
    decay_bias_base,
    decay_shift,
    decay_spike,
    correction_rate_down,
    correction_rate_up,
    correction_rate_base,
):
    query_matrix_rows = jnp.dot(normed_rows, query_matrix, preferred_element_type=jnp.float32)
    key_matrix_rows = jnp.dot(normed_rows, key_matrix, preferred_element_type=jnp.float32)
    value_matrix_rows = jnp.dot(normed_rows, value_matrix, preferred_element_type=jnp.float32)
    decay_low = jnp.tanh(
        jnp.dot(normed_rows, decay_down_factor, preferred_element_type=jnp.float32)
    ).astype(jnp.bfloat16)
    decay_logits = (
        decay_bias_base
        + jnp.dot(decay_low, decay_up_factor, preferred_element_type=jnp.float32)
        + decay_shift
    )
    logarithm_decay = decay_spike - jnp.exp(-jax.nn.softplus(-decay_logits) - 0.5)
    iclr_low = jnp.dot(
        normed_rows, correction_rate_down, preferred_element_type=jnp.float32
    ).astype(jnp.bfloat16)
    learning = jax.nn.sigmoid(
        correction_rate_base
        + jnp.dot(iclr_low, correction_rate_up, preferred_element_type=jnp.float32)
    )
    return (query_matrix_rows, key_matrix_rows, value_matrix_rows, logarithm_decay, learning)


def dot_nn(left, right):
    return lax.dot_general(
        left, right, (((1,), (0,)), ((), ())), preferred_element_type=jnp.float32
    )


def dot_nt(left, right):
    return lax.dot_general(
        left, right, (((1,), (1,)), ((), ())), preferred_element_type=jnp.float32
    )


def dot_tn(left, right):
    return lax.dot_general(
        left, right, (((0,), (0,)), ((), ())), preferred_element_type=jnp.float32
    )


def half_sums(values):
    lane = lax.broadcasted_iota(jnp.int32, values.shape, 1)
    total = jnp.zeros_like(values)
    for head in range(values.shape[1] // HEAD):
        inside = (lane // HEAD) == head
        part = jnp.sum(jnp.where(inside, values, 0.0), axis=1, keepdims=True)
        total = jnp.where(inside, part, total)
    return total


def unit_lower_inverse(below):
    size = below[0].shape[0]
    row = lax.broadcasted_iota(jnp.int32, (size, size), 0)
    column = lax.broadcasted_iota(jnp.int32, (size, size), 1)
    eye = jnp.where(row == column, 1.0, 0.0)
    width = 1
    inverse = None
    while width < size:
        corner = (
            (row // (2 * width) == column // (2 * width))
            & ((row // width) % 2 == 1)
            & ((column // width) % 2 == 0)
        )
        off = [jnp.where(corner, block, 0.0) for block in below]
        if inverse is None:
            inverse = [eye + block for block in off]
        else:
            narrow = [block.astype(jnp.bfloat16) for block in inverse]
            middle = [
                dot_nn(block.astype(jnp.bfloat16), right).astype(jnp.bfloat16)
                for block, right in zip(off, narrow)
            ]
            inverse = [
                whole + dot_nn(left, right)
                for whole, left, right in zip(inverse, narrow, middle)
            ]
        width *= 2
    return [block.astype(jnp.bfloat16) for block in inverse]


def mixer_kernel(q_ref, k_ref, v_ref, decay_ref, rate_ref, local_ref, query_ref, final_ref):
    rows, lanes = q_ref.shape
    heads = lanes // HEAD
    size = min(CHUNK, rows)
    chunks = rows // size
    row = lax.broadcasted_iota(jnp.int32, (size, 2 * size), 0)
    column = lax.broadcasted_iota(jnp.int32, (size, 2 * size), 1) % size
    strict = row > column
    upto = row >= column
    triangle = jnp.where(
        lax.broadcasted_iota(jnp.int32, (size, size), 0)
        >= lax.broadcasted_iota(jnp.int32, (size, size), 1),
        1.0,
        0.0,
    )
    keys = k_ref[...]
    unit = keys * lax.rsqrt(half_sums(keys * keys) + unit_eps)
    erase = -unit
    write = unit * rate_ref[...]
    bf16 = jnp.bfloat16
    per_chunk = []
    for chunk in range(chunks):
        span = slice(chunk * size, (chunk + 1) * size)
        log_decay = decay_ref[span, :]
        cumulative = lax.dot_general(
            triangle,
            log_decay,
            (((1,), (0,)), ((), ())),
            precision=highest,
            preferred_element_type=jnp.float32,
        )
        last = cumulative[size - 1 : size, :]
        middle = 0.5 * last
        fall = jnp.exp(cumulative - middle)
        fall_before = jnp.exp(cumulative - log_decay - middle)
        rise = jnp.exp(middle - cumulative)
        half_fade = jnp.exp(middle)
        e_row = fall_before * erase[span]
        q_row = fall * q_ref[span, :]
        w_row = rise * write[span]
        k_row = rise * keys[span]
        per_chunk.append(
            dict(
                left=jnp.concatenate([e_row, q_row], axis=0).astype(bf16),
                right=jnp.concatenate([w_row, k_row], axis=0).astype(bf16),
                start=jnp.concatenate([e_row * half_fade, q_row * half_fade], axis=0).astype(bf16),
                end=jnp.concatenate([w_row * half_fade, k_row * half_fade], axis=0).astype(bf16),
                fade=jnp.exp(last),
            )
        )
    tables = {}
    for chunk in range(chunks):
        for head in range(heads):
            at = slice(head * HEAD, (head + 1) * HEAD)
            tables[chunk, head] = dot_nt(
                per_chunk[chunk]["left"][:, at], per_chunk[chunk]["right"][:, at]
            )
    order = sorted(tables)
    erase_tables = {key: jnp.where(strict, tables[key][:size], 0.0) for key in order}
    query_tables = {key: jnp.where(upto, tables[key][size:], 0.0).astype(bf16) for key in order}
    inverses = dict(
        zip(order, unit_lower_inverse([erase_tables[key][:, :size] for key in order]))
    )
    pad = jnp.zeros((size, HEAD), jnp.float32)
    carried = [
        jnp.where(
            lax.broadcasted_iota(jnp.int32, (2 * HEAD, HEAD), 0)
            == lax.broadcasted_iota(jnp.int32, (2 * HEAD, HEAD), 1) + HEAD,
            1.0,
            0.0,
        )
        for _ in range(heads)
    ]
    for chunk in range(chunks):
        span = slice(chunk * size, (chunk + 1) * size)
        work = per_chunk[chunk]
        outs = []
        for head in range(heads):
            at = slice(head * HEAD, (head + 1) * HEAD)
            values = jnp.concatenate([v_ref[span, at], pad], axis=1)
            from_start = dot_nt(work["start"][:, at], carried[head].astype(bf16))
            right_side = from_start[:size] + dot_nn(
                erase_tables[chunk, head].astype(bf16),
                jnp.concatenate([jnp.zeros_like(values), values], axis=0).astype(bf16),
            )
            held = dot_nn(inverses[chunk, head], right_side.astype(bf16))
            both = jnp.concatenate([held, values], axis=0).astype(bf16)
            outs.append(from_start[size:] + dot_nn(query_tables[chunk, head], both))
            carried[head] = carried[head] * work["fade"][:, at] + dot_tn(both, work["end"][:, at])
        local_ref[span, :] = jnp.concatenate([out[:, :HEAD] for out in outs], axis=1)
        query_ref[span, :] = jnp.concatenate([out[:, HEAD:] for out in outs], axis=1).astype(bf16)
    final_ref[...] = jnp.concatenate(carried, axis=1).astype(bf16)[None]


def mixer_local(query, keys, values, log_decay, rate, interpret=False):
    rows, channels = query.shape
    lanes = min(PAIR * HEAD, channels)
    steps = channels // lanes
    block = pl.BlockSpec((rows, lanes), lambda i: (0, i))
    return pl.pallas_call(
        mixer_kernel,
        grid=(steps,),
        in_specs=[block] * 5,
        out_specs=[block, block, pl.BlockSpec((1, 2 * HEAD, lanes), lambda i: (i, 0, 0))],
        out_shape=[
            jax.ShapeDtypeStruct((rows, channels), jnp.float32),
            jax.ShapeDtypeStruct((rows, channels), jnp.bfloat16),
            jax.ShapeDtypeStruct((steps, 2 * HEAD, lanes), jnp.bfloat16),
        ],
        cost_estimate=pl.CostEstimate(
            flops=rows * channels * 4096, bytes_accessed=rows * channels * 26, transcendentals=0
        ),
        name="mixer_local",
        interpret=interpret,
    )(query, keys, values, log_decay, rate)


def finish_kernel(place_ref, maps_ref, local_ref, query_ref, gain_ref, out_ref):
    steps, double, lanes = maps_ref.shape[1:]
    heads = lanes // HEAD
    bf16 = jnp.bfloat16
    same = (
        lax.broadcasted_iota(jnp.int32, (lanes, lanes), 0) // HEAD
        == lax.broadcasted_iota(jnp.int32, (lanes, lanes), 1) // HEAD
    )

    def hop(k, states):
        after = []
        for step in range(steps):
            moved = maps_ref[k, step, HEAD:, :]
            square = jnp.where(same, jnp.concatenate([moved] * heads, axis=0), 0).astype(bf16)
            high = states[step].astype(bf16)
            low = (states[step] - high.astype(jnp.float32)).astype(bf16)
            after.append(
                dot_nn(high, square)
                + dot_nn(low, square)
                + maps_ref[k, step, :HEAD, :].astype(jnp.float32)
            )
        return tuple(after)

    states = lax.fori_loop(
        0, place_ref[0], hop, tuple(jnp.zeros((HEAD, lanes), jnp.float32) for _ in range(steps))
    )
    for step in range(steps):
        at = slice(step * lanes, (step + 1) * lanes)
        square = jnp.where(same, jnp.concatenate([states[step]] * heads, axis=0), 0.0).astype(bf16)
        outputs = local_ref[:, at] + dot_nt(query_ref[:, at], square)
        centered = outputs - half_sums(outputs) * (1.0 / HEAD)
        variance = half_sums(centered * centered) * (1.0 / HEAD)
        scaled = centered * lax.rsqrt(variance + group_eps)
        out_ref[:, at] = (scaled * gain_ref[:, at].astype(jnp.float32)).astype(bf16)


def mixer_finish(place, maps, local, query, gain, interpret=False):
    vmem = pl.BlockSpec(memory_space=pltpu.VMEM)
    return pl.pallas_call(
        finish_kernel,
        in_specs=[pl.BlockSpec(memory_space=pltpu.SMEM)] + [vmem] * 4,
        out_specs=vmem,
        out_shape=jax.ShapeDtypeStruct(local.shape, jnp.bfloat16),
        cost_estimate=pl.CostEstimate(
            flops=local.size * 2048, bytes_accessed=maps.size * 2, transcendentals=0
        ),
        name="mixer_finish",
        interpret=interpret,
    )(place, maps, local, query, gain)


def slot_positions(route_block, experts):
    flat_ids = route_block.reshape(-1)
    onehot = (flat_ids[:, None] == jnp.arange(experts, dtype=jnp.int32)[None, :]).astype(jnp.int32)
    earlier_count = jnp.cumsum(onehot, axis=0) - onehot
    return jnp.sum(earlier_count * onehot, axis=1).reshape(route_block.shape)


def per_device(
    mixer_input,
    mixer_gain,
    query_matrix,
    key_matrix,
    value_matrix,
    decay_down_factor,
    decay_up_factor,
    decay_bias_base,
    decay_shift,
    decay_spike,
    correction_rate_down,
    correction_rate_up,
    correction_rate_base,
    head_norm_gain,
    output_weight,
    feedforward_input,
    feedforward_gain,
    routed_expert_index,
    routed_expert_weight,
    expert_gate_weight,
    expert_up_weight,
    expert_down_weight,
    shared_gate_weight,
    shared_up_weight,
    shared_down_weight,
):
    tp_size = lax.axis_size("tp")
    ep_size = lax.axis_size("ep")
    normed_first = rms_rows(mixer_input, mixer_gain)
    (
        query_matrix_rows,
        key_matrix_rows,
        value_matrix_rows,
        logarithm_decay,
        learning,
    ) = mixer_channel_rows(
        normed_first,
        query_matrix,
        key_matrix,
        value_matrix,
        decay_down_factor,
        decay_up_factor,
        decay_bias_base,
        decay_shift,
        decay_spike,
        correction_rate_down,
        correction_rate_up,
        correction_rate_base,
    )
    local, query_map, final = mixer_local(
        query_matrix_rows, key_matrix_rows, value_matrix_rows, logarithm_decay, learning
    )
    maps = lax.all_gather(final, "ep")
    mixed_rows = mixer_finish(
        lax.axis_index("ep").reshape(1), maps, local, query_map, head_norm_gain[None]
    )
    mixed_a = lax.psum_scatter(
        jnp.dot(mixed_rows, output_weight, preferred_element_type=jnp.float32).astype(jnp.bfloat16),
        "tp",
        scatter_dimension=0,
        tiled=True,
    )
    own_count = feedforward_input.shape[0]
    local_count = expert_gate_weight.shape[0]
    experts = local_count * ep_size
    capacity = max(2, 3 * own_count * TOP // (2 * experts))
    normed_own = rms_rows(feedforward_input, feedforward_gain)
    model_width = normed_own.shape[1]
    group_rows = lax.all_gather(normed_own, "tp", axis=0, tiled=True)
    own_ids = lax.dynamic_slice_in_dim(
        routed_expert_index, lax.axis_index("tp") * own_count, own_count, 0
    )
    own_positions = slot_positions(own_ids, experts)
    zero_row = jnp.zeros((1, model_width), jnp.bfloat16)
    slot_index = own_ids * capacity + own_positions
    slot_table = jnp.full((experts * capacity,), own_count, jnp.int32)
    slot_table = slot_table.at[slot_index.reshape(-1)].set(
        jnp.broadcast_to(jnp.arange(own_count, dtype=jnp.int32)[:, None], slot_index.shape).reshape(
            -1
        )
    )
    padded = jnp.concatenate([normed_own, zero_row], axis=0)
    outgoing = padded[slot_table].reshape(experts, capacity, model_width)
    received = lax.all_to_all(outgoing, "ep", split_axis=0, concat_axis=0, tiled=True)
    arrived = lax.all_gather(received[None], "tp", axis=0, tiled=True)
    arrived = arrived.reshape(tp_size, ep_size, local_count, capacity, model_width)
    gate_out = jnp.einsum(
        "tgjcd,jdf->tgjcf", arrived, expert_gate_weight, preferred_element_type=jnp.float32
    )
    up_out = jnp.einsum(
        "tgjcd,jdf->tgjcf", arrived, expert_up_weight, preferred_element_type=jnp.float32
    )
    hidden = (jax.nn.silu(gate_out) * up_out).astype(jnp.bfloat16)
    shared_hidden = (
        jax.nn.silu(jnp.dot(group_rows, shared_gate_weight, preferred_element_type=jnp.float32))
        * jnp.dot(group_rows, shared_up_weight, preferred_element_type=jnp.float32)
    ).astype(jnp.bfloat16)
    shared_hidden = shared_hidden.reshape(tp_size, own_count, -1)
    routed_rows = ep_size * local_count * capacity
    block_rows = routed_rows + own_count
    block_total = lax.axis_size("tp") * block_rows // block_rows
    routed_part = jnp.einsum(
        "tgjcf,jfd->tgjcd", hidden, expert_down_weight, preferred_element_type=jnp.float32
    )
    shared_part = jnp.einsum(
        "tnf,fd->tnd", shared_hidden, shared_down_weight, preferred_element_type=jnp.float32
    )
    joined = jnp.concatenate(
        [routed_part.reshape(block_total, routed_rows, model_width), shared_part], axis=1
    )
    summed = lax.psum_scatter(
        joined.reshape(lax.axis_size("tp") * block_rows, model_width).astype(jnp.bfloat16),
        "tp",
        scatter_dimension=0,
        tiled=True,
    ).astype(jnp.float32)
    expert_out = (
        summed[:routed_rows]
        .astype(jnp.bfloat16)
        .reshape(ep_size, local_count * capacity, model_width)
    )
    returned = lax.all_to_all(expert_out, "ep", split_axis=0, concat_axis=0, tiled=True).reshape(
        experts * capacity, model_width
    )
    picked = returned[own_ids * capacity + own_positions]
    routed = jnp.einsum(
        "rk,rkd->rd", routed_expert_weight, picked.astype(jnp.float32), precision=highest
    )
    mixed_b = (routed + summed[routed_rows:]).astype(jnp.bfloat16)
    return (mixed_a, mixed_b)


def solution(mesh):
    in_specs = (
        P("ep", None),
        P(),
        P(None, "tp"),
        P(None, "tp"),
        P(None, "tp"),
        P(),
        P(None, "tp"),
        P("tp"),
        P("ep", "tp"),
        P("ep", "tp"),
        P(),
        P(None, "tp"),
        P("tp"),
        P("tp"),
        P("tp", None),
        P(("ep", "tp"), None),
        P(),
        P("ep", None),
        P(("ep", "tp"), None),
        P("ep", None, "tp"),
        P("ep", None, "tp"),
        P("ep", "tp", None),
        P(None, "tp"),
        P(None, "tp"),
        P("tp", None),
    )
    out_specs = (P(("ep", "tp"), None), P(("ep", "tp"), None))
    return jax.shard_map(
        per_device, mesh=mesh, in_specs=in_specs, out_specs=out_specs, check_vma=False
    )
```

time: 562 us -> 224 us (0.40); the launches traced: 555 us -> 223 us
  matrix products: 236 us -> 30.2 us
  other arithmetic: 104 us -> 8.93 us
  waiting for transfers between devices: 30.4 us -> 82 us
  local copies, waits for them, and re-layouts: 71 us -> 31.1 us
  blocking collectives: 69.7 us -> 32.8 us
  loops' own time: 17.9 us -> 0 us
  Pallas kernels: 0 us -> 16.8 us
    dot_general x76 -> x0, matrix products: 195 us -> none  [the longest x4 29.1 us: block_tables(): jnp.einsum('htc,htsc,hsc->hts', query_matrix_rows, fade_upto, key_matrix_...]
    another operation x29 -> x0, other arithmetic: 82 us -> none  [the longest x20 81.8 us: block_tables(): jax.scipy.linalg.solve_triangular(identity - erase_write, identity, lower...]
    all_gather x2 -> x0, blocking collectives: 69.7 us -> none  [entering(): lax.all_gather(part.astype(kind), axis)]
    all_to_all x0 -> x1, blocking collectives: none -> 32.8 us  [per_device(): lax.all_to_all(outgoing, 'ep', split_axis=0, concat_axis=0, tiled=True)]
    all_gather x0 -> x1, waiting for transfers between devices: none -> 24.8 us  [per_device(): maps = lax.all_gather(final, 'ep')]
    all_gather x1, waiting for transfers between devices: 0.01 us -> 23.3 us  [per_device(): arrived = lax.all_gather(received[None], 'tp', axis=0, tiled=True)]
    reduce_scatter x1, waiting for transfers between devices: 0.02 us -> 18.9 us  [per_device(): lax.psum_scatter(joined.reshape(lax.axis_size('tp') * block_rows, model_w...]
    another operation x4 -> x0, loops' own time: 17.9 us -> none  [the longest x1 17 us: per_device(): lax.map(lambda block_items: block_tables(*block_items), (to_blocks(query_...]
  transfers between devices with their start and end apart: 6 -> 6, of which waited for: 2 -> 4; matrix products, arithmetic and copies ran while one was open for 67% -> 14% of each run, Pallas kernels for 0% -> 8%
where the time goes in v1:
time: 224 us; the launch traced here: 223 us
  waiting for transfers between devices  82 us (37%)
  blocking collectives  32.8 us (15%)
  local copies, waits for them, and re-layouts  31.1 us (14%)
  matrix products  30.2 us (13%)
  Pallas kernels  16.8 us (8%)
  between operations  15.5 us (7%)
  other arithmetic  8.93 us (4%)
  starting transfers between devices  5.71 us (3%)
    all_to_all x1, blocking collectives, per_device(): lax.all_to_all(outgoing, 'ep', split_axis=0, concat_axis=0, tiled=True)  32.8 us
    all_gather x1, waiting for transfers between devices, per_device(): maps = lax.all_gather(final, 'ep')  24.8 us
    all_gather x1, waiting for transfers between devices, per_device(): arrived = lax.all_gather(received[None], 'tp', axis=0, tiled=True)  23.3 us
    reduce_scatter x1, waiting for transfers between devices, per_device(): lax.psum_scatter(joined.reshape(lax.axis_size('tp') * block_rows, model_w...  18.9 us
    reduce_scatter x1, waiting for transfers between devices, per_device(): lax.psum_scatter(jnp.dot(mixed_rows, output_weight, preferred_element_typ...  15 us
    pallas_call x1, Pallas kernels, mixer_local(): pl.pallas_call(mixer_kernel, grid=(steps,), in_specs=[block] * 5, out_spe...  14.3 us
    dot_general x1, matrix products, per_device(): jnp.einsum('tgjcf,jfd->tgjcd', hidden, expert_down_weight, preferred_elem...  7.94 us
    reshape x1, local copies, waits for them, and re-layouts, per_device(): arrived.reshape(tp_size, ep_size, local_count, capacity, model_width)  6 us
  transfers between devices with their start and end apart: 6, of which 4 were waited for; matrix products, arithmetic and copies ran while one was open for 14% of the time, Pallas kernels for 8%

profile of v1, /device:TPU:0, one launch (start us, length us, event | category | flops | bytes accessed | tf_op | source)
XLA Modules:
  0.0 223.2 jit_solution(4557866522651720523)
XLA Ops:
  10.0 1.8 fusion.48
  15.8 2.0 gather_fusion
  19.1 32.8 %all_to_all.10 = bf16[16,12,2048]{2,1,0:T(8,128)(2,1)S(1)} all-to-all(bf16[16,12,2048]{2,1,0:T(8,128)(2,1)S(1)} %reshape.90), channel_id=1, replica_groups=mesh['ep'=8,'tp'=4] {'ep'}, dimensions={0} | all-to-all | bytes 1572864 | tf_op jit(solution)/shard_map/all_to_all | solution.py:379
  53.4 1.8 fusion.70
  57.7 23.3 %all-gather.10.cloned.1.call-done = bf16[64,12,2048]{2,0,1:T(8,128)(2,1)} async-done(((bf16[16,12,2048]{2,0,1:T(8,128)(2,1)}), bf16[64,12,2048]{2,0,1:T(8,128)(2,1)}) %all-gather.10.cloned.1.call-update) | async-done | bytes 3145744 | tf_op jit(solution)/shard_map/all_gather | solution.py:380
  81.0 6.0 %reshape.91 = bf16[4,8,2,12,2048]{4,2,1,0,3:T(2,128)(2,1)} reshape(bf16[64,12,2048]{2,0,1:T(8,128)(2,1)} %all-gather.10.cloned.1.call-done) | data formatting | bytes 6291456 | tf_op jit(solution)/shard_map/reshape | solution.py:381
  87.0 5.5 %fusion.7 = f32[4,8,2,12,256]{4,3,1,0,2:T(8,128)} fusion(bf16[2,2048,256]{2,1,0:T(8,128)(2,1)} %param.44, bf16[4,8,2,12,2048]{4,2,1,0,3:T(2,128)(2,1)} %reshape.91), kind=kOutput, calls=%fused_computation.14 | convolution fusion | flops 805306368 | bytes 6029312 | tf_op jit(solution)/shard_map/tgjcd,jdf->tgjcf/dot_general | solution.py:382
  92.5 7.9 %convert_bitcast_fusion = bf16[4,8,2,12,2048]{4,3,1,0,2:T(8,128)(2,1)} fusion(bf16[2,256,2048]{2,1,0:T(8,128)(2,1)S(1)} %copy-done, bf16[2,2048,256]{2,1,0:T(8,128)(2,1)} %param.45, bf16[4,8,2,12,2048]{4,2,1,0,3:T(2,128)(2,1)} %reshape.91, f32[4,8,2,12,256]{4,3,1,0,2:T(8,128)} %fusion.7), kind=kOutput, calls=%fused_computation.8 | convolution fusion | flops 1613365248 | bytes 11272192 | tf_op jit(solution)/shard_map/tgjcf,jfd->tgjcd/dot_general | solution.py:397
  100.4 4.9 %copy.44 = bf16[4,8,2,12,2048]{4,0,3,2,1:T(4,128)(2,1)S(1)} copy(bf16[4,8,2,12,2048]{4,3,1,0,2:T(8,128)(2,1)} %convert_bitcast_fusion) | data formatting | bytes 6291456 | tf_op jit(solution)/shard_map/tgjcf,jfd->tgjcd/transpose | solution.py:397
  105.3 2.7 %pad_maximum_fusion = bf16[4,256,2048]{2,0,1:T(4,128)(2,1)S(1)} fusion(bf16[4,64,2048]{2,0,1:T(4,128)(2,1)S(1)} %copy.45, bf16[4,192,2048]{2,0,1:T(4,128)(2,1)S(1)} %bitcast.74), kind=kLoop, calls=%fused_computation.7 | loop fusion | flops 2097152 | bytes 8388608 | tf_op jit(solution)/shard_map/concatenate | solution.py:403
  108.0 4.5 %copy.46 = bf16[4,256,2048]{2,1,0:T(8,128)(2,1)} copy(bf16[4,256,2048]{2,0,1:T(4,128)(2,1)S(1)} %pad_maximum_fusion) | data formatting | bytes 8388608 | tf_op jit(solution)/shard_map/concatenate | solution.py:403
  113.7 1.4 fusion.30.rate_ref
  115.1 2.6 %fusion.54.decay_ref = f32[128,512]{1,0:T(8,128)} fusion(f32[128,512]{1,0:T(8,128)S(1)} %copy-done.12, f32[128,512]{1,0:T(8,128)} %param.33, bf16[64,512]{1,0:T(8,128)(2,1)S(1)} %copy-done.14, bf16[2048,64]{0,1:T(8,128)(2,1)} %param.30, f32[512]{0:T(512)S(1)} %copy-done.16, bf16[128,2048]{1,0:T(8,128)(2,1)S(1)} %copy-done.1, ...), kind=kOutput, calls=%fused_computation.52 | convolution fusion | flops 43786240 | bytes 1649152 | tf_op jit(solution)/shard_map/dot_general | solution.py:48
  117.7 3.1 %fusion.64.v_ref = f32[128,512]{1,0:T(8,128)} fusion(bf16[2048,512]{1,0:T(8,128)(2,1)} %param.29, bf16[128,2048]{1,0:T(8,128)(2,1)S(1)} %copy-done.1, f32[2048]{0:T(1024)S(1)} %convert_element_type.47, f32[128]{0:T(128)S(1)} %add_rsqrt_fusion.1), kind=kOutput, calls=%fused_computation.69 | convolution fusion | flops 269484032 | bytes 2892288 | tf_op jit(solution)/shard_map/dot_general | solution.py:42
  124.1 14.3 %mixer_local.1 = (f32[128,512]{1,0:T(8,128)}, bf16[128,512]{1,0:T(8,128)(2,1)}, bf16[4,128,128]{2,1,0:T(8,128)(2,1)}) custom-call(f32[128,512]{1,0:T(8,128)} %fusion.68.q_ref, f32[128,512]{1,0:T(8,128)} %fusion.66.k_ref, f32[128,512]{1,0:T(8,128)} %fusion.64.v_ref, f32[128,512]{1,0:T(8,128)} %fusion.54.decay_ref, f32[128,512]{1,0:T(8,128)} %fusion.30.rate_ref), custom_call_target="tpu_custom_call" | custom-call | flops 268435456 | bytes 1703936 | tf_op jit(solution)/shard_map/mixer_local/pallas_call | solution.py:219
  138.5 18.9 %reduce-scatter.5.cloned.1.call-done = bf16[256,2048]{1,0:T(8,128)(2,1)} async-done(((bf16[1024,2048]{1,0:T(8,128)(2,1)}), bf16[256,2048]{1,0:T(8,128)(2,1)}) %reduce-scatter.5.cloned.1.call-update) | async-done | bytes 1048592 | tf_op jit(solution)/shard_map/reduce_scatter | solution.py:406
  157.3 2.1 slice.17
  159.4 5.5 %all-to-all-start.1 = ((bf16[8,24,2048]{2,1,0:T(8,128)(2,1)}), bf16[8,24,2048]{2,1,0:T(8,128)(2,1)S(1)}, u32[]{:S(2)}, u32[]{:S(2)}) async-start(bf16[8,24,2048]{2,1,0:T(8,128)(2,1)} %bitcast.75), calls=%async_computation.3 | async-start | bytes 1572864 | tf_op jit(solution)/shard_map/all_to_all | solution.py:417
  165.6 24.8 %all-gather.8.cloned.1.call-done = bf16[32,128,128]{2,1,0:T(8,128)(2,1)} async-done(((bf16[4,128,128]{2,1,0:T(8,128)(2,1)}), bf16[32,128,128]{2,1,0:T(8,128)(2,1)}) %all-gather.8.cloned.1.call-update) | async-done | bytes 1048592 | tf_op jit(solution)/shard_map/all_gather | solution.py:348
  190.4 2.5 %mixer_finish.1 = bf16[128,512]{1,0:T(8,128)(2,1)} custom-call(s32[1]{0:T(128)} %bitcast.place_ref, bf16[8,4,128,128]{3,2,1,0:T(8,128)(2,1)} %bitcast.76, f32[128,512]{1,0:T(8,128)} %get-tuple-element.6.local_ref, bf16[128,512]{1,0:T(8,128)(2,1)} %get-tuple-element.7.query_ref, bf16[1,512]{1,0:T(2,128)(2,1)} %broadcast_in_dim.12.gain_ref), custom_call_target="tpu_custom_call" | custom-call | flops 134217728 | bytes 1048576 | tf_op jit(solution)/shard_map/mixer_finish/pallas_call | solution.py:275
  192.9 2.9 %convolution_convert_fusion.1 = bf16[128,2048]{1,0:T(8,128)(2,1)} fusion(bf16[128,512]{1,0:T(8,128)(2,1)} %mixer_finish.1, bf16[512,2048]{1,0:T(8,128)(2,1)} %param.39), kind=kOutput, calls=%fused_computation.10 | convolution fusion | flops 268697600 | bytes 2752512 | tf_op jit(solution)/shard_map/dot_general | solution.py:353
  197.4 1.8 fusion.71
  199.2 1.8 fusion.49
  201.0 15.0 %reduce-scatter.3.cloned.1.call-done = bf16[32,2048]{1,0:T(8,128)(2,1)} async-done(((bf16[128,2048]{1,0:T(8,128)(2,1)}), bf16[32,2048]{1,0:T(8,128)(2,1)}) %reduce-scatter.3.cloned.1.call-update) | async-done | bytes 131088 | tf_op jit(solution)/shard_map/reduce_scatter | solution.py:352
  (81 shorter events, 17.8 us)
Async XLA Ops:
  8.0 84.5 %copy-start = (bf16[2,256,2048]{2,1,0:T(8,128)(2,1)S(1)}, bf16[2,256,2048]{2,1,0:T(8,128)(2,1)}, u32[]{:S(2)}) copy-start(bf16[2,256,2048]{2,1,0:T(8,128)(2,1)} %param.46) | copy-start | bytes 6291460
  8.0 45.3 %all-gather.6.cloned.1.call-start = ((), (), s32[]{:S(2)}) async-start(), calls=%async_computation.5 | async-start | bytes 1310720 | tf_op jit(solution)/shard_map/all_gather | solution.py:364
  11.8 69.2 %all-gather.10.cloned.1.call-start = ((), (), s32[]{:S(2)}) async-start(), calls=%async_computation.8 | async-start | bytes 3932160 | tf_op jit(solution)/shard_map/all_gather | solution.py:380
  51.9 1.4 copy-start.4
  53.3 104.1 %reduce-scatter.5.cloned.1.call-start = ((), (), s32[]{:S(2)}) async-start(), calls=%async_computation.6 | async-start | bytes 5242880 | tf_op jit(solution)/shard_map/reduce_scatter | solution.py:406
  53.4 1.8 copy-start.6
  53.4 1.8 copy-start.10
  55.2 1.2 copy-start.5
  112.5 0.7 copy-start.7
  112.5 1.1 copy-start.1
  112.5 1.3 copy-start.11
  112.5 1.3 copy-start.13
  112.5 1.3 copy-start.15
  112.5 2.6 %copy-start.12 = (f32[128,512]{1,0:T(8,128)S(1)}, f32[128,512]{1,0:T(8,128)}, u32[]{:S(2)}) copy-start(f32[128,512]{1,0:T(8,128)} %param.34) | copy-start | bytes 786436
  112.5 2.6 %copy-start.14 = (bf16[64,512]{1,0:T(8,128)(2,1)S(1)}, bf16[64,512]{1,0:T(8,128)(2,1)}, u32[]{:S(2)}) copy-start(bf16[64,512]{1,0:T(8,128)(2,1)} %param.31) | copy-start | bytes 196612
  112.5 2.6 %copy-start.16 = (f32[512]{0:T(512)S(1)}, f32[512]{0:T(512)}, u32[]{:S(2)}) copy-start(f32[512]{0:T(512)} %param.32) | copy-start | bytes 6148
  112.6 77.8 %all-gather.8.cloned.1.call-start = ((), (), s32[]{:S(2)}) async-start(), calls=%async_computation.7 | async-start | bytes 1179648 | tf_op jit(solution)/shard_map/all_gather | solution.py:348
  117.7 3.1 %copy-start.2 = (bf16[2048,512]{1,0:T(8,128)(2,1)S(1)}, bf16[2048,512]{1,0:T(8,128)(2,1)}, u32[]{:S(2)}) copy-start(bf16[2048,512]{1,0:T(8,128)(2,1)} %param.28) | copy-start | bytes 6291460
  120.7 2.2 copy-start.3
  124.1 40.9 %copy-start.8 = (bf16[512]{0:T(512)(128)(2,1)S(1)}, bf16[512]{0:T(512)(128)(2,1)}, u32[]{:S(2)}) copy-start(bf16[512]{0:T(512)(128)(2,1)} %param.38) | copy-start | bytes 3076
  159.4 36.7 %all-to-all-start.1 = ((bf16[8,24,2048]{2,1,0:T(8,128)(2,1)}), bf16[8,24,2048]{2,1,0:T(8,128)(2,1)S(1)}, u32[]{:S(2)}, u32[]{:S(2)}) async-start(bf16[8,24,2048]{2,1,0:T(8,128)(2,1)} %bitcast.75), calls=%async_computation.3 | async-start | bytes 1572864 | tf_op jit(solution)/shard_map/all_to_all | solution.py:417
  164.9 51.1 %reduce-scatter.3.cloned.1.call-start = ((), (), s32[]{:S(2)}) async-start(), calls=%async_computation.4 | async-start | bytes 655360 | tf_op jit(solution)/shard_map/reduce_scatter | solution.py:352
  190.4 5.6 %copy-start.9 = (f32[64,2]{0,1:T(2,128)S(1)}, f32[64,2]{0,1:T(2,128)}, u32[]{:S(2)}) copy-start(f32[64,2]{0,1:T(2,128)} %param.43) | copy-start | bytes 1540
Sparse Core Ops, SparseCore 0:
  11.9 19.4 all-gather.5
  53.4 27.5 all-gather.9
  112.6 44.6 reduce-scatter.4
  196.0 20.0 reduce-scatter.2
Sparse Core Ops, SparseCore 1:
  138.5 51.8 all-gather.7

commit v2 on v1

--- a/solution.py
+++ b/solution.py
@@ -1,3 +1,5 @@
+import functools
+
 import jax
 import jax.numpy as jnp
 from jax import lax
@@ -234,10 +236,45 @@
     )(query, keys, values, log_decay, rate)
 
 
-def finish_kernel(place_ref, maps_ref, local_ref, query_ref, gain_ref, out_ref):
-    steps, double, lanes = maps_ref.shape[1:]
+def finish_kernel(
+    size, own_ref, local_ref, query_ref, gain_ref, out_ref, maps_ref, send_sems, recv_sems
+):
+    steps, double, lanes = own_ref.shape
     heads = lanes // HEAD
     bf16 = jnp.bfloat16
+    me = lax.axis_index("ep")
+    barrier = pltpu.get_barrier_semaphore()
+    for ahead in range(1, size):
+        pl.semaphore_signal(
+            barrier,
+            inc=1,
+            device_id={"ep": lax.rem(me + ahead, size)},
+            device_id_type=pl.DeviceIdType.MESH,
+        )
+    pl.semaphore_wait(barrier, size - 1)
+
+    def copy_of(ahead):
+        return pltpu.make_async_remote_copy(
+            src_ref=own_ref,
+            dst_ref=maps_ref.at[ahead],
+            send_sem=send_sems.at[ahead],
+            recv_sem=recv_sems.at[ahead],
+            device_id={"ep": lax.rem(me + ahead, size)},
+            device_id_type=pl.DeviceIdType.MESH,
+        )
+
+    for ahead in range(1, size):
+
+        @pl.when(me + ahead < size)
+        def _():
+            copy_of(ahead).start()
+
+    for ahead in range(1, size):
+
+        @pl.when(me >= ahead)
+        def _():
+            copy_of(ahead).wait_recv()
+
     same = (
         lax.broadcasted_iota(jnp.int32, (lanes, lanes), 0) // HEAD
         == lax.broadcasted_iota(jnp.int32, (lanes, lanes), 1) // HEAD
@@ -246,19 +283,19 @@
     def hop(k, states):
         after = []
         for step in range(steps):
-            moved = maps_ref[k, step, HEAD:, :]
+            moved = maps_ref[me - k, step, HEAD:, :]
             square = jnp.where(same, jnp.concatenate([moved] * heads, axis=0), 0).astype(bf16)
             high = states[step].astype(bf16)
             low = (states[step] - high.astype(jnp.float32)).astype(bf16)
             after.append(
                 dot_nn(high, square)
                 + dot_nn(low, square)
-                + maps_ref[k, step, :HEAD, :].astype(jnp.float32)
+                + maps_ref[me - k, step, :HEAD, :].astype(jnp.float32)
             )
         return tuple(after)
 
     states = lax.fori_loop(
-        0, place_ref[0], hop, tuple(jnp.zeros((HEAD, lanes), jnp.float32) for _ in range(steps))
+        0, me, hop, tuple(jnp.zeros((HEAD, lanes), jnp.float32) for _ in range(steps))
     )
     for step in range(steps):
         at = slice(step * lanes, (step + 1) * lanes)
@@ -269,27 +306,47 @@
         scaled = centered * lax.rsqrt(variance + group_eps)
         out_ref[:, at] = (scaled * gain_ref[:, at].astype(jnp.float32)).astype(bf16)
 
-
-def mixer_finish(place, maps, local, query, gain, interpret=False):
+    for ahead in range(1, size):
+
+        @pl.when(me + ahead < size)
+        def _():
+            copy_of(ahead).wait_send()
+
+
+def mixer_finish(final, local, query, gain):
+    size = lax.axis_size("ep")
     vmem = pl.BlockSpec(memory_space=pltpu.VMEM)
     return pl.pallas_call(
-        finish_kernel,
-        in_specs=[pl.BlockSpec(memory_space=pltpu.SMEM)] + [vmem] * 4,
+        functools.partial(finish_kernel, size),
+        in_specs=[vmem] * 4,
         out_specs=vmem,
         out_shape=jax.ShapeDtypeStruct(local.shape, jnp.bfloat16),
+        scratch_shapes=[
+            pltpu.VMEM((size,) + final.shape, jnp.bfloat16),
+            pltpu.SemaphoreType.DMA((size,)),
+            pltpu.SemaphoreType.DMA((size,)),
+        ],
+        compiler_params=pltpu.CompilerParams(collective_id=0, has_side_effects=True),
         cost_estimate=pl.CostEstimate(
-            flops=local.size * 2048, bytes_accessed=maps.size * 2, transcendentals=0
+            flops=final.size * 4096, bytes_accessed=final.size * size * 16, transcendentals=0
         ),
         name="mixer_finish",
-        interpret=interpret,
-    )(place, maps, local, query, gain)
-
-
-def slot_positions(route_block, experts):
-    flat_ids = route_block.reshape(-1)
-    onehot = (flat_ids[:, None] == jnp.arange(experts, dtype=jnp.int32)[None, :]).astype(jnp.int32)
-    earlier_count = jnp.cumsum(onehot, axis=0) - onehot
-    return jnp.sum(earlier_count * onehot, axis=1).reshape(route_block.shape)
+    )(final, local, query, gain)
+
+
+def slot_choices(route_block, experts, capacity):
+    own_count, top = route_block.shape
+    slot = jnp.arange(experts * capacity, dtype=jnp.int32)[None, :]
+    chosen = [route_block[:, k : k + 1] == slot // capacity for k in range(top)]
+    either = chosen[0]
+    for more in chosen[1:]:
+        either = either | more
+    earlier = jnp.tri(own_count, k=-1, dtype=jnp.bfloat16)
+    position = jnp.dot(
+        earlier, either.astype(jnp.bfloat16), preferred_element_type=jnp.float32
+    ).astype(jnp.int32)
+    here = position == slot % capacity
+    return [choice & here for choice in chosen]
 
 
 def per_device(
@@ -345,16 +402,6 @@
     local, query_map, final = mixer_local(
         query_matrix_rows, key_matrix_rows, value_matrix_rows, logarithm_decay, learning
     )
-    maps = lax.all_gather(final, "ep")
-    mixed_rows = mixer_finish(
-        lax.axis_index("ep").reshape(1), maps, local, query_map, head_norm_gain[None]
-    )
-    mixed_a = lax.psum_scatter(
-        jnp.dot(mixed_rows, output_weight, preferred_element_type=jnp.float32).astype(jnp.bfloat16),
-        "tp",
-        scatter_dimension=0,
-        tiled=True,
-    )
     own_count = feedforward_input.shape[0]
     local_count = expert_gate_weight.shape[0]
     experts = local_count * ep_size
@@ -365,62 +412,74 @@
     own_ids = lax.dynamic_slice_in_dim(
         routed_expert_index, lax.axis_index("tp") * own_count, own_count, 0
     )
-    own_positions = slot_positions(own_ids, experts)
-    zero_row = jnp.zeros((1, model_width), jnp.bfloat16)
-    slot_index = own_ids * capacity + own_positions
-    slot_table = jnp.full((experts * capacity,), own_count, jnp.int32)
-    slot_table = slot_table.at[slot_index.reshape(-1)].set(
-        jnp.broadcast_to(jnp.arange(own_count, dtype=jnp.int32)[:, None], slot_index.shape).reshape(
-            -1
-        )
-    )
-    padded = jnp.concatenate([normed_own, zero_row], axis=0)
-    outgoing = padded[slot_table].reshape(experts, capacity, model_width)
-    received = lax.all_to_all(outgoing, "ep", split_axis=0, concat_axis=0, tiled=True)
-    arrived = lax.all_gather(received[None], "tp", axis=0, tiled=True)
-    arrived = arrived.reshape(tp_size, ep_size, local_count, capacity, model_width)
-    gate_out = jnp.einsum(
-        "tgjcd,jdf->tgjcf", arrived, expert_gate_weight, preferred_element_type=jnp.float32
-    )
-    up_out = jnp.einsum(
-        "tgjcd,jdf->tgjcf", arrived, expert_up_weight, preferred_element_type=jnp.float32
-    )
+    choices = slot_choices(own_ids, experts, capacity)
+    taken = choices[0]
+    weighted = jnp.where(choices[0], routed_expert_weight[:, :1], 0.0)
+    for k in range(1, TOP):
+        taken = taken | choices[k]
+        weighted = weighted + jnp.where(choices[k], routed_expert_weight[:, k : k + 1], 0.0)
+    outgoing = lax.dot_general(
+        taken.astype(jnp.bfloat16),
+        normed_own,
+        (((0,), (0,)), ((), ())),
+        preferred_element_type=jnp.float32,
+    ).astype(jnp.bfloat16)
+    peer_rows = local_count * capacity
+    received = lax.all_to_all(
+        outgoing.reshape(ep_size, peer_rows, model_width), "ep", split_axis=0, concat_axis=0, tiled=True
+    ).reshape(ep_size * peer_rows, model_width)
+    final, received = lax.optimization_barrier((final, received))
+    mixed_rows = mixer_finish(final, local, query_map, head_norm_gain[None])
+    mixed_share = jnp.dot(mixed_rows, output_weight, preferred_element_type=jnp.float32).astype(
+        jnp.bfloat16
+    )
+    routed_rows = ep_size * peer_rows
+    arrived = lax.all_gather(received, "tp", axis=0, tiled=True)
+    arrived, mixed_share = lax.optimization_barrier((arrived, mixed_share))
+    mixed_a = lax.psum_scatter(mixed_share, "tp", scatter_dimension=0, tiled=True)
+    owner = (jnp.arange(tp_size * routed_rows, dtype=jnp.int32) % peer_rows // capacity)[:, None]
+    gate_out = jnp.dot(arrived, expert_gate_weight[0], preferred_element_type=jnp.float32)
+    up_out = jnp.dot(arrived, expert_up_weight[0], preferred_element_type=jnp.float32)
+    for j in range(1, local_count):
+        gate_out = jnp.where(
+            owner == j,
+            jnp.dot(arrived, expert_gate_weight[j], preferred_element_type=jnp.float32),
+            gate_out,
+        )
+        up_out = jnp.where(
+            owner == j,
+            jnp.dot(arrived, expert_up_weight[j], preferred_element_type=jnp.float32),
+            up_out,
+        )
     hidden = (jax.nn.silu(gate_out) * up_out).astype(jnp.bfloat16)
+    hidden = jnp.concatenate(
+        [jnp.where(owner == j, hidden, jnp.zeros_like(hidden)) for j in range(local_count)], axis=1
+    )
     shared_hidden = (
         jax.nn.silu(jnp.dot(group_rows, shared_gate_weight, preferred_element_type=jnp.float32))
         * jnp.dot(group_rows, shared_up_weight, preferred_element_type=jnp.float32)
     ).astype(jnp.bfloat16)
     shared_hidden = shared_hidden.reshape(tp_size, own_count, -1)
-    routed_rows = ep_size * local_count * capacity
     block_rows = routed_rows + own_count
-    block_total = lax.axis_size("tp") * block_rows // block_rows
-    routed_part = jnp.einsum(
-        "tgjcf,jfd->tgjcd", hidden, expert_down_weight, preferred_element_type=jnp.float32
+    down_matrix = expert_down_weight.reshape(-1, model_width)
+    routed_part = jnp.dot(hidden, down_matrix, preferred_element_type=jnp.float32).astype(
+        jnp.bfloat16
     )
     shared_part = jnp.einsum(
         "tnf,fd->tnd", shared_hidden, shared_down_weight, preferred_element_type=jnp.float32
-    )
+    ).astype(jnp.bfloat16)
     joined = jnp.concatenate(
-        [routed_part.reshape(block_total, routed_rows, model_width), shared_part], axis=1
+        [routed_part.reshape(tp_size, routed_rows, model_width), shared_part], axis=1
     )
     summed = lax.psum_scatter(
-        joined.reshape(lax.axis_size("tp") * block_rows, model_width).astype(jnp.bfloat16),
-        "tp",
-        scatter_dimension=0,
-        tiled=True,
-    ).astype(jnp.float32)
-    expert_out = (
-        summed[:routed_rows]
-        .astype(jnp.bfloat16)
-        .reshape(ep_size, local_count * capacity, model_width)
-    )
+        joined.reshape(tp_size * block_rows, model_width), "tp", scatter_dimension=0, tiled=True
+    )
+    expert_out = summed[:routed_rows].reshape(ep_size, peer_rows, model_width)
     returned = lax.all_to_all(expert_out, "ep", split_axis=0, concat_axis=0, tiled=True).reshape(
         experts * capacity, model_width
     )
-    picked = returned[own_ids * capacity + own_positions]
-    routed = jnp.einsum(
-        "rk,rkd->rd", routed_expert_weight, picked.astype(jnp.float32), precision=highest
-    )
+    routed = jnp.dot(weighted, returned.astype(jnp.float32), precision=lax.Precision.HIGH)
+    summed = summed.astype(jnp.float32)
     mixed_b = (routed + summed[routed_rows:]).astype(jnp.bfloat16)
     return (mixed_a, mixed_b)
 

time: 224 us -> 184 us (0.82)
  blocking collectives: 32.8 us -> 0 us
  local copies, waits for them, and re-layouts: 31.1 us -> 6.64 us
  Pallas kernels: 16.8 us -> 37.1 us
  starting transfers between devices: 5.71 us -> 13.1 us
  waiting for transfers between devices: 82 us -> 77.1 us
  other arithmetic: 8.93 us -> 6.28 us
    all_gather x2 -> x1, waiting for transfers between devices: 48 us -> 0.05 us  [per_device(): arrived = lax.all_gather(received, 'tp', axis=0, tiled=True)]
    all_to_all x1 -> x0, blocking collectives: 32.8 us -> none  [per_device(): lax.all_to_all(outgoing, 'ep', split_axis=0, concat_axis=0, tiled=True)]
    reduce_scatter x2, waiting for transfers between devices: 33.9 us -> 56.9 us  [the longest x1 53.4 us: per_device(): lax.psum_scatter(joined.reshape(tp_size * block_rows, model_width), 'tp',...]
    pallas_call x1, Pallas kernels: 2.52 us -> 22.8 us  [mixer_finish(): pl.pallas_call(functools.partial(finish_kernel, size), in_specs=[vmem] *...]
    all_to_all x1, waiting for transfers between devices: 0.01 us -> 19.5 us  [per_device(): lax.all_to_all(expert_out, 'ep', split_axis=0, concat_axis=0, tiled=True)]
    reshape x5 -> x0, local copies, waits for them, and re-layouts: 7.66 us -> none  [the longest x1 6 us: per_device(): arrived.reshape(tp_size, ep_size, local_count, capacity, model_width)]
    all_to_all x0 -> x1, starting transfers between devices: none -> 7.41 us  [per_device(): lax.all_to_all(outgoing.reshape(ep_size, peer_rows, model_width), 'ep', s...]
    concatenate x2 -> x0, local copies, waits for them, and re-layouts: 5.46 us -> none  [the longest x1 4.49 us: per_device(): jnp.concatenate([routed_part.reshape(block_total, routed_rows, model_widt...]
  transfers between devices with their start and end apart: 6 -> 6, of which waited for: 4 -> 3; matrix products, arithmetic and copies ran while one was open for 14% -> 12% of each run, Pallas kernels for 8% -> 20%
where the time goes in v2:
time: 184 us; the launch traced here: 183 us
  waiting for transfers between devices  77.1 us (42%)
  Pallas kernels  37.1 us (20%)
  matrix products  28.9 us (16%)
  between operations  14.1 us (8%)
  starting transfers between devices  13.1 us (7%)
  local copies, waits for them, and re-layouts  6.64 us (4%)
  other arithmetic  6.28 us (3%)
    reduce_scatter x1, waiting for transfers between devices, per_device(): lax.psum_scatter(joined.reshape(tp_size * block_rows, model_width), 'tp',...  53.4 us
    pallas_call x1, Pallas kernels, mixer_finish(): pl.pallas_call(functools.partial(finish_kernel, size), in_specs=[vmem] *...  22.8 us
    all_to_all x1, waiting for transfers between devices, per_device(): lax.all_to_all(expert_out, 'ep', split_axis=0, concat_axis=0, tiled=True)  19.5 us
    pallas_call x1, Pallas kernels, mixer_local(): pl.pallas_call(mixer_kernel, grid=(steps,), in_specs=[block] * 5, out_spe...  14.3 us
    all_to_all x1, starting transfers between devices, per_device(): lax.all_to_all(outgoing.reshape(ep_size, peer_rows, model_width), 'ep', s...  7.41 us
    all_to_all x1, starting transfers between devices, per_device(): lax.all_to_all(expert_out, 'ep', split_axis=0, concat_axis=0, tiled=True)  5.51 us
  transfers between devices with their start and end apart: 6, of which 3 were waited for; matrix products, arithmetic and copies ran while one was open for 12% of the time, Pallas kernels for 20%

profile of v2, /device:TPU:0, one launch (start us, length us, event | category | flops | bytes accessed | tf_op | source)
XLA Modules:
  0.0 183.2 jit_solution(10688187031183963085)
XLA Ops:
  8.1 1.1 fusion.29
  9.2 1.8 fusion.31
  12.1 2.3 %convolution_convert_fusion.2 = bf16[192,2048]{1,0:T(8,128)(2,1)} fusion(bf16[64,2048]{1,0:T(8,128)(2,1)} %fusion.31, pred[64,192]{1,0:T(32,128)(4,1)S(1)} %fusion.11, s32[192]{0:T(256)S(1)} %get-tuple-element.23, s32[64]{0:T(128)S(1)} %get-tuple-element.21, s32[64]{0:T(128)S(1)} %get-tuple-element.20), kind=kOutput, calls=%fused_computation.3 | convolution fusion | flops 50786304 | bytes 1062144 | tf_op jit(solution)/shard_map/dot_general | solution.py:421
  14.4 7.4 %all-to-all-start = ((bf16[8,24,2048]{2,1,0:T(8,128)(2,1)}), bf16[8,24,2048]{2,1,0:T(8,128)(2,1)S(1)}, u32[]{:S(2)}, u32[]{:S(2)}) async-start(bf16[8,24,2048]{2,1,0:T(8,128)(2,1)} %bitcast.57), calls=%async_computation | async-start | bytes 1572864 | tf_op jit(solution)/shard_map/all_to_all | solution.py:428
  22.1 2.2 %fusion.6.rate_ref = f32[128,512]{1,0:T(8,128)} fusion(bf16[64,512]{1,0:T(8,128)(2,1)S(1)} %copy-done.15, bf16[2048,64]{0,1:T(8,128)(2,1)} %param.35, f32[512]{0:T(512)S(1)} %copy-done.16, bf16[128,2048]{1,0:T(8,128)(2,1)S(1)} %copy-done.1, f32[2048]{0:T(1024)S(1)} %convert_element_type.54, f32[128]{0:T(128)S(1)} %add_rsqrt_fusion.1), kind=kOutput, calls=%fused_computation.18 | convolution fusion | flops 43261952 | bytes 1124864 | tf_op jit(solution)/shard_map/dot_general | solution.py:59
  24.3 2.6 %fusion.35.decay_ref = f32[128,512]{1,0:T(8,128)} fusion(f32[128,512]{1,0:T(8,128)} %param.34, f32[128,512]{1,0:T(8,128)} %param.33, bf16[64,512]{1,0:T(8,128)(2,1)} %param.31, bf16[2048,64]{0,1:T(8,128)(2,1)} %param.30, f32[512]{0:T(512)S(1)} %copy-done.17, bf16[128,2048]{1,0:T(8,128)(2,1)S(1)} %copy-done.1, f32[2048]{0:T(1024)S(1)} %convert_element_type.54, ...), kind=kOutput, calls=%fused_computation.56 | convolution fusion | flops 43786240 | bytes 1649152 | tf_op jit(solution)/shard_map/dot_general | solution.py:50
  26.9 3.0 %fusion.69.q_ref = f32[128,512]{1,0:T(8,128)} fusion(bf16[2048,512]{1,0:T(8,128)(2,1)} %param.27, bf16[128,2048]{1,0:T(8,128)(2,1)S(1)} %copy-done.1, f32[2048]{0:T(1024)S(1)} %convert_element_type.54, f32[128]{0:T(128)S(1)} %add_rsqrt_fusion.1), kind=kOutput, calls=%fused_computation.108 | convolution fusion | flops 269484032 | bytes 2892288 | tf_op jit(solution)/shard_map/dot_general | solution.py:42
  29.8 1.2 fusion.67.k_ref
  31.5 1.2 fusion.65.v_ref
  32.7 14.3 %mixer_local.1 = (f32[128,512]{1,0:T(8,128)}, bf16[128,512]{1,0:T(8,128)(2,1)}, bf16[4,128,128]{2,1,0:T(8,128)(2,1)}) custom-call(f32[128,512]{1,0:T(8,128)} %fusion.69.q_ref, f32[128,512]{1,0:T(8,128)} %fusion.67.k_ref, f32[128,512]{1,0:T(8,128)} %fusion.65.v_ref, f32[128,512]{1,0:T(8,128)} %fusion.35.decay_ref, f32[128,512]{1,0:T(8,128)} %fusion.6.rate_ref), custom_call_target="tpu_custom_call" | custom-call | flops 268435456 | bytes 1703936 | tf_op jit(solution)/shard_map/mixer_local/pallas_call | solution.py:221
  48.6 22.8 %mixer_finish.1 = bf16[128,512]{1,0:T(8,128)(2,1)} custom-call(bf16[4,128,128]{2,1,0:T(8,128)(2,1)} %get-tuple-element.11.own_ref, f32[128,512]{1,0:T(8,128)} %get-tuple-element.12.local_ref, bf16[128,512]{1,0:T(8,128)(2,1)} %get-tuple-element.13.query_ref, bf16[1,512]{1,0:T(2,128)(2,1)} %broadcast_in_dim.59.gain_ref), custom_call_target="tpu_custom_call" | custom-call | flops 268435456 | bytes 8388608 | tf_op jit(solution)/shard_map/mixer_finish/pallas_call | solution.py:319
  71.5 2.9 %convolution_convert_fusion.3 = bf16[128,2048]{1,0:T(8,128)(2,1)} fusion(bf16[128,512]{1,0:T(8,128)(2,1)} %mixer_finish.1, bf16[512,2048]{1,0:T(8,128)(2,1)} %param.39), kind=kOutput, calls=%fused_computation.4 | convolution fusion | flops 268697600 | bytes 2752512 | tf_op jit(solution)/shard_map/dot_general | solution.py:433
  74.4 1.8 fusion.71
  78.0 3.3 %fusion.17 = f32[768,256]{0,1:T(8,128)S(1)} fusion(bf16[768,2048]{1,0:T(8,128)(2,1)} %all-gather.3.cloned.1.call-done, bf16[2,2048,256]{2,1,0:T(8,128)(2,1)} %param.45), kind=kOutput, calls=%fused_computation.33 | convolution fusion | flops 805306368 | bytes 4980736 | tf_op jit(solution)/shard_map/dot_general | solution.py:451
  82.9 1.1 convolution_select_fusion.1
  84.5 1.2 broadcast_select_fusion.1
  85.7 1.8 %convolution_convert_fusion = bf16[768,2048]{1,0:T(8,128)(2,1)S(1)} fusion(bf16[512,2048]{1,0:T(8,128)(2,1)S(1)} %bitcast.54, bf16[768,256]{0,1:T(8,128)(2,1)S(1)} %get-tuple-element.17, bf16[768,256]{0,1:T(8,128)(2,1)S(1)} %get-tuple-element.16), kind=kOutput, calls=%fused_computation.1 | convolution fusion | flops 1613758464 | bytes 6029312 | tf_op jit(solution)/shard_map/dot_general | solution.py:465
  87.6 2.3 %pad_maximum_fusion = bf16[4,256,2048]{2,1,0:T(8,128)(2,1)} fusion(bf16[4,64,2048]{2,1,0:T(8,128)(2,1)S(1)} %convolution_convert_fusion.1, bf16[4,192,2048]{2,1,0:T(8,128)(2,1)S(1)} %bitcast.60), kind=kLoop, calls=%fused_computation | loop fusion | flops 8388608 | bytes 8388608 | tf_op jit(solution)/shard_map/concatenate | solution.py:471
  89.9 53.4 %reduce-scatter.5.cloned.1.call-done = bf16[256,2048]{1,0:T(8,128)(2,1)} async-done(((bf16[1024,2048]{1,0:T(8,128)(2,1)}), bf16[256,2048]{1,0:T(8,128)(2,1)}) %reduce-scatter.5.cloned.1.call-update) | async-done | bytes 1048592 | tf_op jit(solution)/shard_map/reduce_scatter | solution.py:474
  143.3 2.1 %slice.44 = bf16[192,2048]{1,0:T(8,128)(2,1)} slice(bf16[256,2048]{1,0:T(8,128)(2,1)} %reduce-scatter.5.cloned.1.call-done), slice={[0:192], [0:2048]} | slice | bytes 1572864 | tf_op jit(solution)/shard_map/slice | solution.py:477
  145.4 5.5 %all-to-all-start.1 = ((bf16[8,24,2048]{2,1,0:T(8,128)(2,1)}), bf16[8,24,2048]{2,1,0:T(8,128)(2,1)S(1)}, u32[]{:S(2)}, u32[]{:S(2)}) async-start(bf16[8,24,2048]{2,1,0:T(8,128)(2,1)} %bitcast.59), calls=%async_computation.3 | async-start | bytes 1572864 | tf_op jit(solution)/shard_map/all_to_all | solution.py:478
  151.5 19.5 %all-to-all-done.1 = bf16[8,24,2048]{2,1,0:T(8,128)(2,1)S(1)} async-done(((bf16[8,24,2048]{2,1,0:T(8,128)(2,1)}), bf16[8,24,2048]{2,1,0:T(8,128)(2,1)S(1)}, u32[]{:S(2)}, u32[]{:S(2)}) %all-to-all-start.1) | async-done | bytes 786464 | tf_op jit(solution)/shard_map/all_to_all | solution.py:478
  171.0 2.1 %fusion = bf16[64,2048]{1,0:T(8,128)(2,1)} fusion(bf16[192,2048]{1,0:T(8,128)(2,1)S(1)} %bitcast.58, bf16[256,2048]{1,0:T(8,128)(2,1)} %reduce-scatter.5.cloned.1.call-done, pred[64,192]{1,0:T(32,128)(4,1)S(1)} %fusion.11, f32[64]{0:T(128)S(1)} %get-tuple-element.19, f32[64]{0:T(128)S(1)} %get-tuple-element.18, s32[192]{0:T(256)S(1)} %get-tuple-element.23, ...), kind=kOutput, calls=%fused_computation.6 | convolution fusion | flops 151474176 | bytes 1324800 | tf_op jit(solution)/shard_map/dot_general | solution.py:481
  173.1 3.5 %reduce-scatter.3.cloned.1.call-done = bf16[32,2048]{1,0:T(8,128)(2,1)} async-done(((bf16[128,2048]{1,0:T(8,128)(2,1)}), bf16[32,2048]{1,0:T(8,128)(2,1)}) %reduce-scatter.3.cloned.1.call-update) | async-done | bytes 131088 | tf_op jit(solution)/shard_map/reduce_scatter | solution.py:439
  (64 shorter events, 8.6 us)
Async XLA Ops:
  7.2 78.6 %copy-start = (bf16[2,256,2048]{2,1,0:T(8,128)(2,1)S(1)}, bf16[2,256,2048]{2,1,0:T(8,128)(2,1)}, u32[]{:S(2)}) copy-start(bf16[2,256,2048]{2,1,0:T(8,128)(2,1)} %param.46) | copy-start | bytes 6291460
  7.2 14.7 %copy-start.8 = (bf16[2048]{0:T(1024)(128)(2,1)S(1)}, bf16[2048]{0:T(1024)(128)(2,1)}, u32[]{:S(2)}) copy-start(bf16[2048]{0:T(1024)(128)(2,1)} %param.26) | copy-start | bytes 12292
  7.2 14.7 %copy-start.1 = (bf16[128,2048]{1,0:T(8,128)(2,1)S(1)}, bf16[128,2048]{1,0:T(8,128)(2,1)}, u32[]{:S(2)}) copy-start(bf16[128,2048]{1,0:T(8,128)(2,1)} %param.25) | copy-start | bytes 1572868
  7.2 67.2 %all-gather.5.cloned.1.call-start = ((), (), s32[]{:S(2)}) async-start(), calls=%async_computation.6 | async-start | bytes 1310720 | tf_op jit(solution)/shard_map/all_gather | solution.py:411
  9.2 12.9 %copy-start.15 = (bf16[64,512]{1,0:T(8,128)(2,1)S(1)}, bf16[64,512]{1,0:T(8,128)(2,1)}, u32[]{:S(2)}) copy-start(bf16[64,512]{1,0:T(8,128)(2,1)} %param.36) | copy-start | bytes 196612
  9.2 12.9 %copy-start.16 = (f32[512]{0:T(512)S(1)}, f32[512]{0:T(512)}, u32[]{:S(2)}) copy-start(f32[512]{0:T(512)} %param.37) | copy-start | bytes 6148
  14.4 9.9 %copy-start.17 = (f32[512]{0:T(512)S(1)}, f32[512]{0:T(512)}, u32[]{:S(2)}) copy-start(f32[512]{0:T(512)} %param.32) | copy-start | bytes 6148
  14.4 32.6 %all-to-all-start = ((bf16[8,24,2048]{2,1,0:T(8,128)(2,1)}), bf16[8,24,2048]{2,1,0:T(8,128)(2,1)S(1)}, u32[]{:S(2)}, u32[]{:S(2)}) async-start(bf16[8,24,2048]{2,1,0:T(8,128)(2,1)} %bitcast.57), calls=%async_computation | async-start | bytes 1572864 | tf_op jit(solution)/shard_map/all_to_all | solution.py:428
  21.8 56.2 %all-gather.3.cloned.1.call-start = ((), (), s32[]{:S(2)}) async-start(), calls=%async_computation.4 | async-start | bytes 3932160 | tf_op jit(solution)/shard_map/all_gather | solution.py:437
  26.9 3.0 %copy-start.3 = (bf16[2048,512]{1,0:T(8,128)(2,1)S(1)}, bf16[2048,512]{1,0:T(8,128)(2,1)}, u32[]{:S(2)}) copy-start(bf16[2048,512]{1,0:T(8,128)(2,1)} %param.28) | copy-start | bytes 6291460
  29.8 1.7 copy-start.4
  31.5 16.5 %copy-start.9 = (bf16[512]{0:T(512)(128)(2,1)S(1)}, bf16[512]{0:T(512)(128)(2,1)}, u32[]{:S(2)}) copy-start(bf16[512]{0:T(512)(128)(2,1)} %param.38) | copy-start | bytes 3076
  47.0 0.9 copy-start.2
  47.9 26.4 %copy-start.5 = (bf16[2048,256]{1,0:T(8,128)(2,1)S(1)}, bf16[2048,256]{1,0:T(8,128)(2,1)}, u32[]{:S(2)}) copy-start(bf16[2048,256]{1,0:T(8,128)(2,1)} %param.47) | copy-start | bytes 3145732
  47.9 95.3 %reduce-scatter.5.cloned.1.call-start = ((), (), s32[]{:S(2)}) async-start(), calls=%async_computation.7 | async-start | bytes 5242880 | tf_op jit(solution)/shard_map/reduce_scatter | solution.py:474
  74.4 1.8 copy-start.7
  74.4 1.9 %copy-start.14 = (bf16[2048,256]{1,0:T(8,128)(2,1)S(1)}, bf16[2048,256]{1,0:T(8,128)(2,1)}, u32[]{:S(2)}) copy-start(bf16[2048,256]{1,0:T(8,128)(2,1)} %param.48) | copy-start | bytes 3145732
  76.3 1.2 copy-start.6
  78.0 3.4 %copy-start.11 = (bf16[768,2048]{1,0:T(8,128)(2,1)S(1)}, bf16[768,2048]{1,0:T(8,128)(2,1)}, u32[]{:S(2)}) copy-start(bf16[768,2048]{1,0:T(8,128)(2,1)} %all-gather.3.cloned.1.call-done) | copy-start | bytes 9437188
  78.0 3.8 %copy-start.12 = (bf16[2,2048,256]{2,1,0:T(8,128)(2,1)S(1)}, bf16[2,2048,256]{2,1,0:T(8,128)(2,1)}, u32[]{:S(2)}) copy-start(bf16[2,2048,256]{2,1,0:T(8,128)(2,1)} %param.44) | copy-start | bytes 6291460
  82.9 1.6 copy-start.13
  89.9 61.6 %copy-start.10 = (f32[64,2]{0,1:T(2,128)S(1)}, f32[64,2]{0,1:T(2,128)}, u32[]{:S(2)}) copy-start(f32[64,2]{0,1:T(2,128)} %param.43) | copy-start | bytes 1540
  145.4 25.6 %all-to-all-start.1 = ((bf16[8,24,2048]{2,1,0:T(8,128)(2,1)}), bf16[8,24,2048]{2,1,0:T(8,128)(2,1)S(1)}, u32[]{:S(2)}, u32[]{:S(2)}) async-start(bf16[8,24,2048]{2,1,0:T(8,128)(2,1)} %bitcast.59), calls=%async_computation.3 | async-start | bytes 1572864 | tf_op jit(solution)/shard_map/all_to_all | solution.py:478
  150.9 25.7 %reduce-scatter.3.cloned.1.call-start = ((), (), s32[]{:S(2)}) async-start(), calls=%async_computation.5 | async-start | bytes 655360 | tf_op jit(solution)/shard_map/reduce_scatter | solution.py:439
Sparse Core Ops, SparseCore 0:
  11.2 19.4 all-gather.4
  48.1 29.8 all-gather.2
  90.0 53.2 reduce-scatter.4
  154.5 22.1 reduce-scatter.2

commit v3 on v2

--- a/solution.py
+++ b/solution.py
@@ -332,6 +332,20 @@
         ),
         name="mixer_finish",
     )(final, local, query, gain)
+
+
+def halving_sum(shares, axis):
+    size, me = lax.axis_size(axis), lax.axis_index(axis)
+    distance = 1
+    while distance < size:
+        bit = (me // distance) % 2
+        pairs = shares.reshape((shares.shape[0] // 2, 2) + shares.shape[1:])
+        kept = lax.dynamic_index_in_dim(pairs, bit, 1, keepdims=False)
+        given = lax.dynamic_index_in_dim(pairs, 1 - bit, 1, keepdims=False)
+        came = lax.ppermute(given, axis, [(i, i ^ distance) for i in range(size)])
+        shares = (kept.astype(jnp.float32) + came.astype(jnp.float32)).astype(jnp.bfloat16)
+        distance *= 2
+    return shares[0]
 
 
 def slot_choices(route_block, experts, capacity):
@@ -436,7 +450,7 @@
     routed_rows = ep_size * peer_rows
     arrived = lax.all_gather(received, "tp", axis=0, tiled=True)
     arrived, mixed_share = lax.optimization_barrier((arrived, mixed_share))
-    mixed_a = lax.psum_scatter(mixed_share, "tp", scatter_dimension=0, tiled=True)
+    mixed_a = halving_sum(mixed_share.reshape(tp_size, -1, model_width), "tp")
     owner = (jnp.arange(tp_size * routed_rows, dtype=jnp.int32) % peer_rows // capacity)[:, None]
     gate_out = jnp.dot(arrived, expert_gate_weight[0], preferred_element_type=jnp.float32)
     up_out = jnp.dot(arrived, expert_up_weight[0], preferred_element_type=jnp.float32)
@@ -471,9 +485,7 @@
     joined = jnp.concatenate(
         [routed_part.reshape(tp_size, routed_rows, model_width), shared_part], axis=1
     )
-    summed = lax.psum_scatter(
-        joined.reshape(tp_size * block_rows, model_width), "tp", scatter_dimension=0, tiled=True
-    )
+    summed = halving_sum(joined, "tp")
     expert_out = summed[:routed_rows].reshape(ep_size, peer_rows, model_width)
     returned = lax.all_to_all(expert_out, "ep", split_axis=0, concat_axis=0, tiled=True).reshape(
         experts * capacity, model_width

time: 184 us -> 171 us (0.929)
  waiting for transfers between devices: 77.1 us -> 44.8 us
  starting transfers between devices: 13.1 us -> 24 us
  other arithmetic: 6.28 us -> 12.3 us
  local copies, waits for them, and re-layouts: 6.64 us -> 8.48 us
    reduce_scatter x2 -> x0, waiting for transfers between devices: 56.9 us -> none  [the longest x1 53.4 us: per_device(): lax.psum_scatter(joined.reshape(tp_size * block_rows, model_width), 'tp',...]
    ppermute x0 -> x4, waiting for transfers between devices: none -> 31.7 us  [halving_sum(): came = lax.ppermute(given, axis, [(i, i ^ distance) for i in range(size)])]
    all_to_all x1, starting transfers between devices: 5.51 us -> 13.2 us  [per_device(): lax.all_to_all(expert_out, 'ep', split_axis=0, concat_axis=0, tiled=True)]
    all_to_all x1, waiting for transfers between devices: 19.5 us -> 12.9 us  [per_device(): lax.all_to_all(expert_out, 'ep', split_axis=0, concat_axis=0, tiled=True)]
    convert_element_type x0 -> x3, other arithmetic: none -> 5.85 us  [halving_sum(): (kept.astype(jnp.float32) + came.astype(jnp.float32)).astype(jnp.bfloat16)]
    ppermute x0 -> x4, starting transfers between devices: none -> 3.38 us  [halving_sum(): came = lax.ppermute(given, axis, [(i, i ^ distance) for i in range(size)])]
    squeeze x0 -> x2, other arithmetic: none -> 2.43 us  [the longest x1 1.74 us: halving_sum(): given = lax.dynamic_index_in_dim(pairs, 1 - bit, 1, keepdims=False)]
    concatenate x1 -> x0, other arithmetic: 2.26 us -> none  [per_device(): jnp.concatenate([routed_part.reshape(tp_size, routed_rows, model_width),...]
  transfers between devices with their start and end apart: 6 -> 8, of which waited for: 3 -> 5; matrix products, arithmetic and copies ran while one was open for 12% -> 14% of each run, Pallas kernels for 20% -> 22%
where the time goes in v3:
time: 171 us; the launch traced here: 170 us
  waiting for transfers between devices  44.8 us (26%)
  Pallas kernels  37.1 us (22%)
  matrix products  29.2 us (17%)
  starting transfers between devices  24 us (14%)
  between operations  14.4 us (8%)
  other arithmetic  12.3 us (7%)
  local copies, waits for them, and re-layouts  8.48 us (5%)
    ppermute x4, waiting for transfers between devices, halving_sum(): came = lax.ppermute(given, axis, [(i, i ^ distance) for i in range(size)])  31.7 us
    pallas_call x1, Pallas kernels, mixer_finish(): pl.pallas_call(functools.partial(finish_kernel, size), in_specs=[vmem] *...  22.8 us
    pallas_call x1, Pallas kernels, mixer_local(): pl.pallas_call(mixer_kernel, grid=(steps,), in_specs=[block] * 5, out_spe...  14.3 us
    all_to_all x1, starting transfers between devices, per_device(): lax.all_to_all(expert_out, 'ep', split_axis=0, concat_axis=0, tiled=True)  13.2 us
    all_to_all x1, waiting for transfers between devices, per_device(): lax.all_to_all(expert_out, 'ep', split_axis=0, concat_axis=0, tiled=True)  12.9 us
    all_to_all x1, starting transfers between devices, per_device(): lax.all_to_all(outgoing.reshape(ep_size, peer_rows, model_width), 'ep', s...  7.41 us
    convert_element_type x3, other arithmetic, halving_sum(): (kept.astype(jnp.float32) + came.astype(jnp.float32)).astype(jnp.bfloat16)  5.85 us
    unnamed x42, local copies, waits for them, and re-layouts  5.07 us
  transfers between devices with their start and end apart: 8, of which 5 were waited for; matrix products, arithmetic and copies ran while one was open for 14% of the time, Pallas kernels for 22%

profile of v3, /device:TPU:0, one launch (start us, length us, event | category | flops | bytes accessed | tf_op | source)
XLA Modules:
  0.0 170.2 jit_solution(10186878676712943005)
XLA Ops:
  9.2 1.8 %fusion.36 = bf16[64,2048]{1,0:T(8,128)(2,1)} fusion(bf16[64,2048]{1,0:T(8,128)(2,1)} %param.40, f32[2048]{0:T(1024)S(1)} %convert_element_type.107, f32[64]{0:T(128)S(1)} %add_rsqrt_fusion), kind=kLoop, calls=%fused_computation.60 | loop fusion | flops 524288 | bytes 532736 | tf_op jit(solution)/shard_map/convert_element_type | solution.py:25
  12.1 2.3 %convolution_convert_fusion.2 = bf16[192,2048]{1,0:T(8,128)(2,1)} fusion(bf16[64,2048]{1,0:T(8,128)(2,1)} %fusion.36, pred[64,192]{1,0:T(32,128)(4,1)S(1)} %fusion.16, s32[192]{0:T(256)S(1)} %get-tuple-element.23, s32[64]{0:T(128)S(1)} %get-tuple-element.21, s32[64]{0:T(128)S(1)} %get-tuple-element.20), kind=kOutput, calls=%fused_computation.8 | convolution fusion | flops 50786304 | bytes 1062144 | tf_op jit(solution)/shard_map/dot_general | solution.py:435
  14.5 7.4 %all-to-all-start = ((bf16[8,24,2048]{2,1,0:T(8,128)(2,1)}), bf16[8,24,2048]{2,1,0:T(8,128)(2,1)S(1)}, u32[]{:S(2)}, u32[]{:S(2)}) async-start(bf16[8,24,2048]{2,1,0:T(8,128)(2,1)} %bitcast.87), calls=%async_computation | async-start | bytes 1572864 | tf_op jit(solution)/shard_map/all_to_all | solution.py:442
  22.2 2.2 %fusion.11.rate_ref = f32[128,512]{1,0:T(8,128)} fusion(bf16[64,512]{1,0:T(8,128)(2,1)S(1)} %copy-done.18, bf16[2048,64]{0,1:T(8,128)(2,1)} %param.35, f32[512]{0:T(512)S(1)} %copy-done.19, bf16[128,2048]{1,0:T(8,128)(2,1)S(1)} %copy-done.2, f32[2048]{0:T(1024)S(1)} %convert_element_type.101, f32[128]{0:T(128)S(1)} %add_rsqrt_fusion.1), kind=kOutput, calls=%fused_computation.28 | convolution fusion | flops 43261952 | bytes 1124864 | tf_op jit(solution)/shard_map/dot_general | solution.py:59
  24.4 2.6 %fusion.41.decay_ref = f32[128,512]{1,0:T(8,128)} fusion(f32[128,512]{1,0:T(8,128)} %param.34, f32[128,512]{1,0:T(8,128)} %param.33, bf16[64,512]{1,0:T(8,128)(2,1)} %param.31, bf16[2048,64]{0,1:T(8,128)(2,1)} %param.30, f32[512]{0:T(512)S(1)} %copy-done.20, bf16[128,2048]{1,0:T(8,128)(2,1)S(1)} %copy-done.2, f32[2048]{0:T(1024)S(1)} %convert_element_type.101, ...), kind=kOutput, calls=%fused_computation.68 | convolution fusion | flops 43786240 | bytes 1649152 | tf_op jit(solution)/shard_map/dot_general | solution.py:50
  26.9 2.9 %fusion.76.q_ref = f32[128,512]{1,0:T(8,128)} fusion(bf16[2048,512]{1,0:T(8,128)(2,1)} %param.27, bf16[128,2048]{1,0:T(8,128)(2,1)S(1)} %copy-done.2, f32[2048]{0:T(1024)S(1)} %convert_element_type.101, f32[128]{0:T(128)S(1)} %add_rsqrt_fusion.1), kind=kOutput, calls=%fused_computation.126 | convolution fusion | flops 269484032 | bytes 2892288 | tf_op jit(solution)/shard_map/dot_general | solution.py:42
  32.8 14.3 %mixer_local.1 = (f32[128,512]{1,0:T(8,128)}, bf16[128,512]{1,0:T(8,128)(2,1)}, bf16[4,128,128]{2,1,0:T(8,128)(2,1)}) custom-call(f32[128,512]{1,0:T(8,128)} %fusion.76.q_ref, f32[128,512]{1,0:T(8,128)} %fusion.74.k_ref, f32[128,512]{1,0:T(8,128)} %fusion.72.v_ref, f32[128,512]{1,0:T(8,128)} %fusion.41.decay_ref, f32[128,512]{1,0:T(8,128)} %fusion.11.rate_ref), custom_call_target="tpu_custom_call" | custom-call | flops 268435456 | bytes 1703936 | tf_op jit(solution)/shard_map/mixer_local/pallas_call | solution.py:221
  48.7 22.8 %mixer_finish.1 = bf16[128,512]{1,0:T(8,128)(2,1)} custom-call(bf16[4,128,128]{2,1,0:T(8,128)(2,1)} %get-tuple-element.11.own_ref, f32[128,512]{1,0:T(8,128)} %get-tuple-element.12.local_ref, bf16[128,512]{1,0:T(8,128)(2,1)} %get-tuple-element.13.query_ref, bf16[1,512]{1,0:T(2,128)(2,1)} %broadcast_in_dim.59.gain_ref), custom_call_target="tpu_custom_call" | custom-call | flops 268435456 | bytes 8388608 | tf_op jit(solution)/shard_map/mixer_finish/pallas_call | solution.py:319
  71.5 3.0 %convolution_convert_fusion.3 = bf16[128,2048]{1,0:T(8,128)(2,1)} fusion(bf16[128,512]{1,0:T(8,128)(2,1)} %mixer_finish.1, bf16[512,2048]{1,0:T(8,128)(2,1)} %param.39), kind=kOutput, calls=%fused_computation.9 | convolution fusion | flops 268697600 | bytes 2752512 | tf_op jit(solution)/shard_map/dot_general | solution.py:447
  74.4 1.8 %fusion.78 = f32[256,256]{1,0:T(8,128)S(1)} fusion(bf16[256,2048]{1,0:T(8,128)(2,1)} %all-gather.5.cloned.1.call-done, bf16[2048,256]{1,0:T(8,128)(2,1)S(1)} %copy-done.8), kind=kOutput, calls=%fused_computation.127 | convolution fusion | flops 268435456 | bytes 2359296 | tf_op jit(solution)/shard_map/dot_general | solution.py:473
  78.1 3.3 %fusion.22 = f32[768,256]{0,1:T(8,128)S(1)} fusion(bf16[768,2048]{1,0:T(8,128)(2,1)} %all-gather.3.cloned.1.call-done, bf16[2,2048,256]{2,1,0:T(8,128)(2,1)} %param.45), kind=kOutput, calls=%fused_computation.43 | convolution fusion | flops 805306368 | bytes 4980736 | tf_op jit(solution)/shard_map/dot_general | solution.py:465
  85.8 1.8 %convolution_convert_fusion = bf16[768,2048]{1,0:T(8,128)(2,1)S(1)} fusion(bf16[512,2048]{1,0:T(8,128)(2,1)S(1)} %bitcast.80, bf16[768,256]{0,1:T(8,128)(2,1)S(1)} %get-tuple-element.17, bf16[768,256]{0,1:T(8,128)(2,1)S(1)} %get-tuple-element.16), kind=kOutput, calls=%fused_computation.6 | convolution fusion | flops 1613758464 | bytes 6029312 | tf_op jit(solution)/shard_map/dot_general | solution.py:479
  87.6 1.7 %fusion.3 = bf16[2,256,2048]{2,1,0:T(8,128)(2,1)} fusion(s32[]{:T(128)S(6)} %select_n.137, bf16[2,2,192,2048]{3,2,1,0:T(8,128)(2,1)S(1)} %bitcast.81, bf16[2,2,64,2048]{3,2,1,0:T(8,128)(2,1)S(1)} %bitcast.83), kind=kLoop, calls=%fused_computation.13 | loop fusion | flops 4194304 | bytes 6291460 | tf_op jit(solution)/shard_map/jit(dynamic_index_in_dim)/squeeze | solution.py:344
  90.1 4.3 %collective-permute-done.2 = bf16[2,256,2048]{2,1,0:T(8,128)(2,1)} collective-permute-done((bf16[2,256,2048]{2,1,0:T(8,128)(2,1)}, bf16[2,256,2048]{2,1,0:T(8,128)(2,1)}, u32[]{:S(2)}, u32[]{:S(2)}) %collective-permute-start.2) | collective-permute-done | bytes 2097184 | tf_op jit(solution)/shard_map/ppermute | solution.py:345
  94.4 2.8 %fusion = bf16[2,256,2048]{2,1,0:T(8,128)(2,1)S(1)} fusion(bf16[2,256,2048]{2,1,0:T(8,128)(2,1)} %collective-permute-done.2, s32[]{:T(128)S(6)} %select_n.136, bf16[2,2,192,2048]{3,2,1,0:T(8,128)(2,1)} %bitcast.82, bf16[2,2,64,2048]{3,2,1,0:T(8,128)(2,1)S(1)} %bitcast.84), kind=kLoop, calls=%fused_computation.5 | loop fusion | flops 8388608 | bytes 8388612 | tf_op jit(solution)/shard_map/convert_element_type | solution.py:346
  97.2 1.3 copy-done.3
  99.6 1.5 collective-permute-start.3
  101.2 24.0 %collective-permute-done.3 = bf16[1,256,2048]{2,1,0:T(8,128)(2,1)} collective-permute-done((bf16[1,256,2048]{2,1,0:T(8,128)(2,1)}, bf16[1,256,2048]{2,1,0:T(8,128)(2,1)}, u32[]{:S(2)}, u32[]{:S(2)}) %collective-permute-start.3) | collective-permute-done | bytes 1048608 | tf_op jit(solution)/shard_map/ppermute | solution.py:345
  125.2 1.9 %add_convert_fusion = bf16[1,256,2048]{2,1,0:T(8,128)(2,1)S(1)} fusion(bf16[1,256,2048]{2,1,0:T(8,128)(2,1)} %collective-permute-done.3, bf16[2,256,2048]{2,1,0:T(8,128)(2,1)} %copy-done.3, s32[]{:T(128)S(6)} %select_n.140), kind=kLoop, calls=%fused_computation.16 | loop fusion | flops 2097152 | bytes 3145732 | tf_op jit(solution)/shard_map/convert_element_type | solution.py:346
  128.2 13.2 %all-to-all-start.1 = ((bf16[8,24,2048]{2,1,0:T(8,128)(2,1)}), bf16[8,24,2048]{2,1,0:T(8,128)(2,1)}, u32[]{:S(2)}, u32[]{:S(2)}) async-start(bf16[8,24,2048]{2,1,0:T(8,128)(2,1)} %bitcast.86), calls=%async_computation.1 | async-start | bytes 1572864 | tf_op jit(solution)/shard_map/all_to_all | solution.py:490
  142.5 1.6 collective-permute-start.1
  144.1 3.4 %collective-permute-done.1 = bf16[1,32,2048]{2,1,0:T(8,128)(2,1)S(1)} collective-permute-done((bf16[1,32,2048]{2,1,0:T(8,128)(2,1)S(1)}, bf16[1,32,2048]{2,1,0:T(8,128)(2,1)S(1)}, u32[]{:S(2)}, u32[]{:S(2)}) %collective-permute-start.1) | collective-permute-done | bytes 131104 | tf_op jit(solution)/shard_map/ppermute | solution.py:345
  148.2 12.9 %all-to-all-done.1 = bf16[8,24,2048]{2,1,0:T(8,128)(2,1)} async-done(((bf16[8,24,2048]{2,1,0:T(8,128)(2,1)}), bf16[8,24,2048]{2,1,0:T(8,128)(2,1)}, u32[]{:S(2)}, u32[]{:S(2)}) %all-to-all-start.1) | async-done | bytes 786464 | tf_op jit(solution)/shard_map/all_to_all | solution.py:490
  161.1 2.3 %fusion.1 = bf16[64,2048]{1,0:T(8,128)(2,1)} fusion(bf16[192,2048]{1,0:T(8,128)(2,1)} %bitcast.22, bf16[1,256,2048]{2,1,0:T(8,128)(2,1)S(1)} %add_convert_fusion, pred[64,192]{1,0:T(32,128)(4,1)S(1)} %fusion.16, f32[64]{0:T(128)S(1)} %get-tuple-element.19, f32[64]{0:T(128)S(1)} %get-tuple-element.18, s32[192]{0:T(256)S(1)} %get-tuple-element.23, ...), kind=kOutput, calls=%fused_computation.11 | convolution fusion | flops 151474176 | bytes 1324800 | tf_op jit(solution)/shard_map/dot_general | solution.py:493
  (79 shorter events, 18.5 us)
Async XLA Ops:
  7.2 78.6 %copy-start = (bf16[2,256,2048]{2,1,0:T(8,128)(2,1)S(1)}, bf16[2,256,2048]{2,1,0:T(8,128)(2,1)}, u32[]{:S(2)}) copy-start(bf16[2,256,2048]{2,1,0:T(8,128)(2,1)} %param.46) | copy-start | bytes 6291460
  7.2 14.7 %copy-start.11 = (bf16[2048]{0:T(1024)(128)(2,1)S(1)}, bf16[2048]{0:T(1024)(128)(2,1)}, u32[]{:S(2)}) copy-start(bf16[2048]{0:T(1024)(128)(2,1)} %param.26) | copy-start | bytes 12292
  7.2 14.7 %copy-start.2 = (bf16[128,2048]{1,0:T(8,128)(2,1)S(1)}, bf16[128,2048]{1,0:T(8,128)(2,1)}, u32[]{:S(2)}) copy-start(bf16[128,2048]{1,0:T(8,128)(2,1)} %param.25) | copy-start | bytes 1572868
  7.2 67.2 %all-gather.5.cloned.1.call-start = ((), (), s32[]{:S(2)}) async-start(), calls=%async_computation.3 | async-start | bytes 1310720 | tf_op jit(solution)/shard_map/all_gather | solution.py:425
  9.2 12.9 %copy-start.18 = (bf16[64,512]{1,0:T(8,128)(2,1)S(1)}, bf16[64,512]{1,0:T(8,128)(2,1)}, u32[]{:S(2)}) copy-start(bf16[64,512]{1,0:T(8,128)(2,1)} %param.36) | copy-start | bytes 196612
  9.2 12.9 %copy-start.19 = (f32[512]{0:T(512)S(1)}, f32[512]{0:T(512)}, u32[]{:S(2)}) copy-start(f32[512]{0:T(512)} %param.37) | copy-start | bytes 6148
  14.5 9.9 %copy-start.20 = (f32[512]{0:T(512)S(1)}, f32[512]{0:T(512)}, u32[]{:S(2)}) copy-start(f32[512]{0:T(512)} %param.32) | copy-start | bytes 6148
  14.5 32.6 %all-to-all-start = ((bf16[8,24,2048]{2,1,0:T(8,128)(2,1)}), bf16[8,24,2048]{2,1,0:T(8,128)(2,1)S(1)}, u32[]{:S(2)}, u32[]{:S(2)}) async-start(bf16[8,24,2048]{2,1,0:T(8,128)(2,1)} %bitcast.87), calls=%async_computation | async-start | bytes 1572864 | tf_op jit(solution)/shard_map/all_to_all | solution.py:442
  21.9 56.2 %all-gather.3.cloned.1.call-start = ((), (), s32[]{:S(2)}) async-start(), calls=%async_computation.2 | async-start | bytes 3932160 | tf_op jit(solution)/shard_map/all_gather | solution.py:451
  26.9 3.0 %copy-start.5 = (bf16[2048,512]{1,0:T(8,128)(2,1)S(1)}, bf16[2048,512]{1,0:T(8,128)(2,1)}, u32[]{:S(2)}) copy-start(bf16[2048,512]{1,0:T(8,128)(2,1)} %param.28) | copy-start | bytes 6291460
  31.6 16.4 %copy-start.12 = (bf16[512]{0:T(512)(128)(2,1)S(1)}, bf16[512]{0:T(512)(128)(2,1)}, u32[]{:S(2)}) copy-start(bf16[512]{0:T(512)(128)(2,1)} %param.38) | copy-start | bytes 3076
  48.0 26.4 %copy-start.8 = (bf16[2048,256]{1,0:T(8,128)(2,1)S(1)}, bf16[2048,256]{1,0:T(8,128)(2,1)}, u32[]{:S(2)}) copy-start(bf16[2048,256]{1,0:T(8,128)(2,1)} %param.47) | copy-start | bytes 3145732
  74.4 1.8 %copy-start.10 = (bf16[256,2048]{1,0:T(8,128)(2,1)S(1)}, bf16[256,2048]{1,0:T(8,128)(2,1)}, u32[]{:S(2)}) copy-start(bf16[256,2048]{1,0:T(8,128)(2,1)} %all-gather.5.cloned.1.call-done) | copy-start | bytes 3145732
  74.4 1.9 %copy-start.17 = (bf16[2048,256]{1,0:T(8,128)(2,1)S(1)}, bf16[2048,256]{1,0:T(8,128)(2,1)}, u32[]{:S(2)}) copy-start(bf16[2048,256]{1,0:T(8,128)(2,1)} %param.48) | copy-start | bytes 3145732
  78.1 3.3 %copy-start.14 = (bf16[768,2048]{1,0:T(8,128)(2,1)S(1)}, bf16[768,2048]{1,0:T(8,128)(2,1)}, u32[]{:S(2)}) copy-start(bf16[768,2048]{1,0:T(8,128)(2,1)} %all-gather.3.cloned.1.call-done) | copy-start | bytes 9437188
  78.1 3.8 %copy-start.15 = (bf16[2,2048,256]{2,1,0:T(8,128)(2,1)S(1)}, bf16[2,2048,256]{2,1,0:T(8,128)(2,1)}, u32[]{:S(2)}) copy-start(bf16[2,2048,256]{2,1,0:T(8,128)(2,1)} %param.44) | copy-start | bytes 6291460
  87.6 2.2 %copy-start.1 = (bf16[768,2048]{1,0:T(8,128)(2,1)}, bf16[768,2048]{1,0:T(8,128)(2,1)S(1)}, u32[]{:S(2)}) copy-start(bf16[768,2048]{1,0:T(8,128)(2,1)S(1)} %convolution_convert_fusion) | copy-start | bytes 9437188
  89.9 4.5 %collective-permute-start.2 = (bf16[2,256,2048]{2,1,0:T(8,128)(2,1)}, bf16[2,256,2048]{2,1,0:T(8,128)(2,1)}, u32[]{:S(2)}, u32[]{:S(2)}) collective-permute-start(bf16[2,256,2048]{2,1,0:T(8,128)(2,1)} %fusion.3), channel_id=1, source_target_pairs={{0,1},{1,0},{2,3},{3,2},{4,5},{5,4},{6,7},{7,6},{8,9},{9,8},{10,11... | collective-permute-start | bytes 6291464 | tf_op jit(solution)/shard_map/ppermute | solution.py:345
  98.6 2.5 %copy-start.7 = (bf16[128,2048]{1,0:T(8,128)(2,1)S(1)}, bf16[128,2048]{1,0:T(8,128)(2,1)}, u32[]{:S(2)}) copy-start(bf16[128,2048]{1,0:T(8,128)(2,1)} %convolution_convert_fusion.3) | copy-start | bytes 1572868
  99.6 25.6 %collective-permute-start.3 = (bf16[1,256,2048]{2,1,0:T(8,128)(2,1)}, bf16[1,256,2048]{2,1,0:T(8,128)(2,1)}, u32[]{:S(2)}, u32[]{:S(2)}) collective-permute-start(bf16[1,256,2048]{2,1,0:T(8,128)(2,1)} %constant_dynamic-slice_fusion), channel_id=1, source_target_pairs={{0,2},{1,3},{2,0},{3,1},{4,6},{5,7},{6,4},{7,5},{8,10},{9,11},{10,... | collective-permute-start | bytes 3145736 | tf_op jit(solution)/shard_map/ppermute | solution.py:345
  101.1 40.2 %collective-permute-start = (bf16[2,32,2048]{2,1,0:T(8,128)(2,1)S(1)}, bf16[2,32,2048]{2,1,0:T(8,128)(2,1)}, u32[]{:S(2)}, u32[]{:S(2)}) collective-permute-start(bf16[2,32,2048]{2,1,0:T(8,128)(2,1)S(1)} %dynamic-slice_bitcast_fusion), channel_id=1, source_target_pairs={{0,1},{1,0},{2,3},{3,2},{4,5},{5,4},{6,7},{7,6},{8,9},{9,8},{10,11... | collective-permute-start | bytes 786440 | tf_op jit(solution)/shard_map/ppermute | solution.py:345
  127.2 16.9 %copy-start.13 = (f32[64,2]{0,1:T(2,128)S(1)}, f32[64,2]{0,1:T(2,128)}, u32[]{:S(2)}) copy-start(f32[64,2]{0,1:T(2,128)} %param.43) | copy-start | bytes 1540
  128.2 33.0 %all-to-all-start.1 = ((bf16[8,24,2048]{2,1,0:T(8,128)(2,1)}), bf16[8,24,2048]{2,1,0:T(8,128)(2,1)}, u32[]{:S(2)}, u32[]{:S(2)}) async-start(bf16[8,24,2048]{2,1,0:T(8,128)(2,1)} %bitcast.86), calls=%async_computation.1 | async-start | bytes 1572864 | tf_op jit(solution)/shard_map/all_to_all | solution.py:490
  142.5 5.0 %collective-permute-start.1 = (bf16[1,32,2048]{2,1,0:T(8,128)(2,1)S(1)}, bf16[1,32,2048]{2,1,0:T(8,128)(2,1)S(1)}, u32[]{:S(2)}, u32[]{:S(2)}) collective-permute-start(bf16[1,32,2048]{2,1,0:T(8,128)(2,1)S(1)} %constant_dynamic-slice_fusion.1), channel_id=1, source_target_pairs={{0,2},{1,3},{2,0},{3,1},{4,6},{5,7},{6,4},{7,5},{8,10},{9,11},{10,... | collective-permute-start | bytes 393224 | tf_op jit(solution)/shard_map/ppermute | solution.py:345
  (5 other events, 6.7 us)
Sparse Core Ops, SparseCore 0:
  11.2 19.4 all-gather.4
  48.1 29.8 all-gather.2
